TPU v7x, 128 devices: a whole 4x4x4 slice. The times are simulated.
128 devices in a mesh: sp: 64 (over z, y, x), tp: 2 (over core).
Axes of the slice: x: 4, y: 4, z: 4, core: 2. Of those that a mesh axis runs over, the one named last changes fastest.
Arguments:
- latent: bfloat16 [16384, 256], P('sp'), may hold values from -6 to 6
- rotary_key: bfloat16 [16384, 64], P('sp'), may hold values from -7 to 7
- doc_ids: int32 [16384], P('sp'), may hold values from 0 to 31, never falling along the last dimension, each value on 1 to 1024 neighbouring positions
- queries_content: bfloat16 [16384, 1024], P('sp', 'tp'), may hold values from -6 to 6
- queries_rotary: bfloat16 [16384, 512], P('sp', 'tp'), may hold values from -400 to 400
- w_key_up: bfloat16 [256, 1024], replicated, may hold values from -0.375 to 0.375
- w_value_up: bfloat16 [256, 1024], replicated, may hold values from -0.375 to 0.375
- w_out: bfloat16 [1024, 2048], P('tp'), may hold values from -1.5 to 1.5
- residual: bfloat16 [16384, 2048], P(('sp', 'tp')), may hold values from -4 to 4
- norm_gain: float32 [2048], replicated, may hold values from 0.1 to 1.9
- routes: int32 [16384, 2], P(('sp', 'tp')), may hold values from 0 to 63, all different within a row; in each aligned block of 128 rows (0 to 127, 128 to 255, ...) at most 8 rows name the same one
- route_weights: float32 [16384, 2], P(('sp', 'tp')), may hold values from 0.1 to 1
- w_gate: bfloat16 [64, 2048, 3584], P('sp', None, 'tp'), may hold values from -0.125 to 0.125
- w_up: bfloat16 [64, 2048, 3584], P('sp', None, 'tp'), may hold values from -0.125 to 0.125
- w_down: bfloat16 [64, 3584, 2048], P('sp', 'tp'), may hold values from -0.09375 to 0.09375
- out_gain: float32 [2048], replicated, may hold values from 0.1 to 1.9
Outputs:
- mixed: bfloat16 [16384, 2048], P(('sp', 'tp'))
Inputs may be any that keep to these rules, and one draw needn't show every extreme that they name: `doc_ids`: document numbers never fall along positions; each document holds 1 to 1024 positions, and one holds exactly 1024. `routes`: each row names 2 different experts; among the rows of one device (aligned blocks of 128 rows) no expert is named more than 8 times, and in some blocks one expert is named exactly 8 times.
All inputs are finite; a program needn't handle non-finite values.
Results may differ from a plain program's by a relative error of at most 0.014.
Values may be sent and summed in bfloat16 or wider, within the bound.
A program may use at most 128 MiB of HBM per device.

v0:
```python
import jax
import jax.numpy as jnp
from jax import lax
from jax.sharding import PartitionSpec as P

HEADS = 8
DK = 128
DR = 64
DV = 128
TOPK = 2
REACH = 4


ROPE_THETA = 500000.0
RESIDUAL_SCALE = 2.0**0.5
NORM_EPSILON = 1e-05


def shifted(value, axis, steps):
    count = lax.axis_size(axis)
    leading, last = (max(0, -steps), min(count, count - steps))
    return lax.ppermute(value, axis, [(source, source + steps) for source in range(leading, last)])


def in_blocks(x, dim, peers):
    lengths = x.shape
    tiles = x.reshape(*lengths[:dim], peers, lengths[dim] // peers, *lengths[dim + 1 :])
    return jnp.moveaxis(tiles, dim, 0)


def sum_at_owner(x, axis, dim):
    peers = lax.axis_size(axis)
    tiles = lax.all_to_all(in_blocks(x, dim, peers), axis, 0, 0, tiled=True)
    return jnp.sum(tiles.astype(jnp.float32), axis=0)


def from_everyone(x, axis):
    peers = lax.axis_size(axis)
    return lax.all_to_all(jnp.broadcast_to(x[None], (peers, *x.shape)), axis, 0, 0, tiled=True)


def joined_along(tiles, dim):
    lengths = list(tiles.shape[1:])
    lengths[dim] *= tiles.shape[0]
    return jnp.moveaxis(tiles, 0, dim).reshape(lengths)


def gather_directly(x, axis, dim):
    tiles = from_everyone(x, axis)
    return joined_along(tiles, dim)


def rotate(values, positions):
    half_width = values.shape[-1] // 2
    frequency = ROPE_THETA ** (-2.0 * jnp.arange(half_width, dtype=jnp.float32) / values.shape[-1])
    angles = positions.astype(jnp.float32)[:, None] * frequency[None, :]
    table_shape = (values.shape[0],) + (1,) * (values.ndim - 2) + (half_width,)
    cosine = jnp.cos(angles).reshape(table_shape)
    sine_part = jnp.sin(angles).reshape(table_shape)
    widened = values.astype(jnp.float32)
    first_half = widened[..., :half_width]
    second = widened[..., half_width:]
    return jnp.concatenate(
        [first_half * cosine - second * sine_part, second * cosine + first_half * sine_part], -1
    )


def layer_norm(values, gain_vec):
    centre = jnp.mean(values, -1, keepdims=True)
    spread = jnp.mean(jnp.square(values - centre), -1, keepdims=True)
    return (values - centre) * lax.rsqrt(spread + NORM_EPSILON) * gain_vec


def per_device(
    latent,
    rotary_key,
    doc_ids,
    queries_content,
    queries_rotary,
    w_key_up,
    w_value_up,
    w_out,
    residual,
    norm_gain,
    routes,
    route_weights,
    w_gate,
    w_up,
    w_down,
    out_gain,
):
    tok_dev = latent.shape[0]
    core_count = lax.axis_size("tp")
    chip_count = lax.axis_size("sp")
    heads_here = HEADS // core_count
    head_index = lax.axis_index("tp")
    sp_index = lax.axis_index("sp")
    key_cols = lax.dynamic_slice_in_dim(w_key_up, head_index * heads_here * DK, heads_here * DK, 1)
    value_cols = lax.dynamic_slice_in_dim(
        w_value_up, head_index * heads_here * DV, heads_here * DV, 1
    )
    own_position = sp_index * tok_dev + jnp.arange(tok_dev, dtype=jnp.int32)
    query_turned = rotate(queries_rotary.reshape(tok_dev, heads_here, DR), own_position).astype(
        jnp.bfloat16
    )
    query_block = queries_content.reshape(tok_dev, heads_here, DK)
    pieces = [(latent, rotary_key, doc_ids)]
    for distance in range(1, REACH + 1):
        pieces.append(shifted((latent, rotary_key, doc_ids), "sp", distance))
    ordered = pieces[::-1]
    key_latent = jnp.concatenate([piece[0] for piece in ordered], 0)
    key_rope = jnp.concatenate([piece[1] for piece in ordered], 0)
    key_doc = jnp.concatenate([piece[2] for piece in ordered], 0)
    key_count = key_latent.shape[0]
    key_position = (sp_index - REACH) * tok_dev + jnp.arange(key_count, dtype=jnp.int32)
    key_content = jnp.dot(key_latent, key_cols, preferred_element_type=jnp.float32).astype(
        jnp.bfloat16
    )
    key_content = key_content.reshape(key_count, heads_here, DK)
    values = jnp.dot(key_latent, value_cols, preferred_element_type=jnp.float32).astype(
        jnp.bfloat16
    )
    values = values.reshape(key_count, heads_here, DV)
    key_turned = rotate(key_rope, key_position).astype(jnp.bfloat16)
    score_scale = (DK + DR) ** (-0.5)
    scores = jnp.einsum(
        "phd,qhd->hpq", query_block, key_content, preferred_element_type=jnp.float32
    )
    scores = scores + jnp.einsum(
        "phd,qd->hpq", query_turned, key_turned, preferred_element_type=jnp.float32
    )
    scores = scores * score_scale
    allowed = (key_position[None, :] <= own_position[:, None]) & (key_position[None, :] >= 0)
    allowed = allowed & (key_doc[None, :] == doc_ids[:, None])
    scores = jnp.where(allowed[None], scores, -jnp.inf)
    row_peak = jnp.max(scores, -1, keepdims=True)
    lifted = jnp.exp(scores - row_peak)
    probability = (lifted / jnp.sum(lifted, -1, keepdims=True)).astype(jnp.bfloat16)
    attended = jnp.einsum("hpq,qhd->phd", probability, values, preferred_element_type=jnp.float32)
    attended = attended.astype(jnp.bfloat16).reshape(tok_dev, heads_here * DV)
    partial_value = jnp.dot(attended, w_out, preferred_element_type=jnp.float32)
    projected = sum_at_owner(
        partial_value.astype(jnp.bfloat16).astype(jnp.float32).astype(jnp.bfloat16), "tp", 0
    )
    normed = layer_norm(
        RESIDUAL_SCALE * residual.astype(jnp.float32) + projected, norm_gain
    ).astype(jnp.bfloat16)
    row_count = normed.shape[0]
    model_width = normed.shape[1]
    capacity = max(2, 2 * row_count * TOPK // chip_count)
    flat_route = routes.reshape(-1)
    member = (flat_route[:, None] == jnp.arange(chip_count, dtype=jnp.int32)[None, :]).astype(
        jnp.int32
    )
    slot_rank = jnp.sum((jnp.cumsum(member, 0) - member) * member, 1)
    slot_index = flat_route * capacity + slot_rank
    placing = (
        slot_index[None, :] == jnp.arange(chip_count * capacity, dtype=jnp.int32)[:, None]
    ).astype(jnp.int32)
    placing = jnp.sum(placing.reshape(chip_count * capacity, row_count, TOPK), -1).astype(
        jnp.bfloat16
    )
    outbound = jnp.dot(placing, normed, preferred_element_type=jnp.float32).astype(jnp.bfloat16)
    outbound = outbound.reshape(chip_count, capacity, model_width)
    landed = lax.all_to_all(outbound, "sp", split_axis=0, concat_axis=0, tiled=True)
    arrived = gather_directly(landed[:, None], "tp", 1)
    flat_rows = arrived.reshape(-1, model_width)
    gate_pre = jnp.dot(flat_rows, w_gate[0], preferred_element_type=jnp.float32)
    upward = jnp.dot(flat_rows, w_up[0], preferred_element_type=jnp.float32)
    hidden = (jax.nn.silu(gate_pre) * upward).astype(jnp.bfloat16)
    partial_value = jnp.dot(hidden, w_down[0], preferred_element_type=jnp.float32)
    partial_value = (
        partial_value.astype(jnp.bfloat16)
        .astype(jnp.float32)
        .reshape(chip_count, core_count, capacity, model_width)
    )
    reduced = sum_at_owner(partial_value.astype(jnp.bfloat16), "tp", 1).astype(jnp.bfloat16)
    returned = lax.all_to_all(
        reduced.reshape(chip_count, capacity, model_width),
        "sp",
        split_axis=0,
        concat_axis=0,
        tiled=True,
    )
    returned = returned.reshape(chip_count * capacity, model_width)
    picked = (
        jnp.take(returned, slot_index, axis=0)
        .reshape(row_count, TOPK, model_width)
        .astype(jnp.float32)
    )
    routed_sum = jnp.sum(picked * route_weights[:, :, None], 1)
    combined = RESIDUAL_SCALE * normed.astype(jnp.float32) + routed_sum
    return layer_norm(combined, out_gain).astype(jnp.bfloat16)


def solution(mesh):
    return jax.shard_map(
        per_device,
        mesh=mesh,
        in_specs=(
            P("sp", None),
            P("sp", None),
            P("sp"),
            P("sp", "tp"),
            P("sp", "tp"),
            P(),
            P(),
            P("tp", None),
            P(("sp", "tp"), None),
            P(),
            P(("sp", "tp"), None),
            P(("sp", "tp"), None),
            P("sp", None, "tp"),
            P("sp", None, "tp"),
            P("sp", "tp", None),
            P(),
        ),
        out_specs=P(("sp", "tp"), None),
        check_vma=False,
    )
```

profile of v0, /device:TPU:12, one launch (start us, length us, event | category | flops | bytes accessed | tf_op | source)
XLA Modules:
  0.0 259.9 jit_solution(459518997331708088)
XLA Ops:
  0.0 3.6 %collective-permute-start = (bf16[256,256]{1,0:T(8,128)(2,1)}, bf16[256,256]{1,0:T(8,128)(2,1)S(1)}, u32[]{:S(2)}, u32[]{:S(2)}) collective-permute-start(bf16[256,256]{1,0:T(8,128)(2,1)} %param.16), channel_id=1, source_target_pairs={{0,8},{2,10},{4,12},{6,14},{8,16},{10,18},{12,20},{14,22},{16,24},... | collective-permute-start | bytes 393224 | tf_op jit(solution)/shard_map/ppermute | solution.py:22
  3.6 3.2 %collective-permute-start.1 = (bf16[256,256]{1,0:T(8,128)(2,1)}, bf16[256,256]{1,0:T(8,128)(2,1)S(1)}, u32[]{:S(2)}, u32[]{:S(2)}) collective-permute-start(bf16[256,256]{1,0:T(8,128)(2,1)} %param.16), channel_id=1, source_target_pairs={{0,6},{2,8},{4,10},{6,12},{8,14},{10,16},{12,18},{14,20},{16,22},{... | collective-permute-start | bytes 393224 | tf_op jit(solution)/shard_map/ppermute | solution.py:22
  6.8 4.6 %collective-permute-start.2 = (bf16[256,256]{1,0:T(8,128)(2,1)}, bf16[256,256]{1,0:T(8,128)(2,1)S(1)}, u32[]{:S(2)}, u32[]{:S(2)}) collective-permute-start(bf16[256,256]{1,0:T(8,128)(2,1)} %param.16), channel_id=1, source_target_pairs={{0,4},{2,6},{4,8},{6,10},{8,12},{10,14},{12,16},{14,18},{16,20},{1... | collective-permute-start | bytes 393224 | tf_op jit(solution)/shard_map/ppermute | solution.py:22
  11.4 2.8 %collective-permute-start.3 = (bf16[256,256]{1,0:T(8,128)(2,1)}, bf16[256,256]{1,0:T(8,128)(2,1)S(1)}, u32[]{:S(2)}, u32[]{:S(2)}) collective-permute-start(bf16[256,256]{1,0:T(8,128)(2,1)} %param.16), channel_id=1, source_target_pairs={{0,2},{2,4},{4,6},{6,8},{8,10},{10,12},{12,14},{14,16},{16,18},{18... | collective-permute-start | bytes 393224 | tf_op jit(solution)/shard_map/ppermute | solution.py:22
  14.2 3.5 %collective-permute-start.4 = (s32[256]{0:T(256)}, s32[256]{0:T(256)S(1)}, u32[]{:S(2)}, u32[]{:S(2)}) collective-permute-start(s32[256]{0:T(256)} %param.18), channel_id=1, source_target_pairs={{0,8},{2,10},{4,12},{6,14},{8,16},{10,18},{12,20},{14,22},{16,24},... | collective-permute-start | bytes 3080 | tf_op jit(solution)/shard_map/ppermute | solution.py:22
  22.8 4.1 %collective-permute-start.5 = (s32[256]{0:T(256)}, s32[256]{0:T(256)S(1)}, u32[]{:S(2)}, u32[]{:S(2)}) collective-permute-start(s32[256]{0:T(256)} %param.18), channel_id=1, source_target_pairs={{0,6},{2,8},{4,10},{6,12},{8,14},{10,16},{12,18},{14,20},{16,22},{... | collective-permute-start | bytes 3080 | tf_op jit(solution)/shard_map/ppermute | solution.py:22
  26.9 2.5 collective-permute-done.5
  29.4 3.9 %collective-permute-start.6 = (s32[256]{0:T(256)}, s32[256]{0:T(256)S(1)}, u32[]{:S(2)}, u32[]{:S(2)}) collective-permute-start(s32[256]{0:T(256)} %param.18), channel_id=1, source_target_pairs={{0,4},{2,6},{4,8},{6,10},{8,12},{10,14},{12,16},{14,18},{16,20},{1... | collective-permute-start | bytes 3080 | tf_op jit(solution)/shard_map/ppermute | solution.py:22
  33.3 3.2 %collective-permute-done.6 = s32[256]{0:T(256)S(1)} collective-permute-done((s32[256]{0:T(256)}, s32[256]{0:T(256)S(1)}, u32[]{:S(2)}, u32[]{:S(2)}) %collective-permute-start.6) | collective-permute-done | bytes 1056 | tf_op jit(solution)/shard_map/ppermute | solution.py:22
  36.6 4.3 %collective-permute-start.7 = (s32[256]{0:T(256)}, s32[256]{0:T(256)S(1)}, u32[]{:S(2)}, u32[]{:S(2)}) collective-permute-start(s32[256]{0:T(256)} %param.18), channel_id=1, source_target_pairs={{0,2},{2,4},{4,6},{6,8},{8,10},{10,12},{12,14},{14,16},{16,18},{18... | collective-permute-start | bytes 3080 | tf_op jit(solution)/shard_map/ppermute | solution.py:22
  42.4 3.5 %collective-permute-start.8 = (bf16[256,64]{0,1:T(8,128)(2,1)}, bf16[256,64]{0,1:T(8,128)(2,1)S(1)}, u32[]{:S(2)}, u32[]{:S(2)}) collective-permute-start(bf16[256,64]{0,1:T(8,128)(2,1)} %param.17), channel_id=1, source_target_pairs={{0,8},{2,10},{4,12},{6,14},{8,16},{10,18},{12,20},{14,22},{16,24},... | collective-permute-start | bytes 98312 | tf_op jit(solution)/shard_map/ppermute | solution.py:22
  48.4 4.8 %collective-permute-start.9 = (bf16[256,64]{0,1:T(8,128)(2,1)}, bf16[256,64]{0,1:T(8,128)(2,1)S(1)}, u32[]{:S(2)}, u32[]{:S(2)}) collective-permute-start(bf16[256,64]{0,1:T(8,128)(2,1)} %param.17), channel_id=1, source_target_pairs={{0,6},{2,8},{4,10},{6,12},{8,14},{10,16},{12,18},{14,20},{16,22},{... | collective-permute-start | bytes 98312 | tf_op jit(solution)/shard_map/ppermute | solution.py:22
  53.2 2.1 collective-permute-done.9
  55.3 7.2 %collective-permute-start.10 = (bf16[256,64]{0,1:T(8,128)(2,1)}, bf16[256,64]{0,1:T(8,128)(2,1)S(1)}, u32[]{:S(2)}, u32[]{:S(2)}) collective-permute-start(bf16[256,64]{0,1:T(8,128)(2,1)} %param.17), channel_id=1, source_target_pairs={{0,4},{2,6},{4,8},{6,10},{8,12},{10,14},{12,16},{14,18},{16,20},{1... | collective-permute-start | bytes 98312 | tf_op jit(solution)/shard_map/ppermute | solution.py:22
  62.5 1.9 collective-permute-done.10
  64.4 7.8 %collective-permute-start.11 = (bf16[256,64]{0,1:T(8,128)(2,1)}, bf16[256,64]{0,1:T(8,128)(2,1)S(1)}, u32[]{:S(2)}, u32[]{:S(2)}) collective-permute-start(bf16[256,64]{0,1:T(8,128)(2,1)} %param.17), channel_id=1, source_target_pairs={{0,2},{2,4},{4,6},{6,8},{8,10},{10,12},{12,14},{14,16},{16,18},{18... | collective-permute-start | bytes 98312 | tf_op jit(solution)/shard_map/ppermute | solution.py:22
  80.1 2.3 copy-done.2
  84.0 6.2 %fusion.17 = bf16[4,128,256]{2,1,0:T(8,128)(2,1)} fusion(bf16[1280,4,128]{0,2,1:T(8,128)(2,1)S(1)} %bitcast.95, f32[4,256]{1,0:T(4,128)S(1)} %exponential_reduce_fusion, f32[4,256,1280]{1,2,0:T(8,128)} %copy-done.2), kind=kOutput, calls=%fused_computation.27 | convolution fusion | flops 339609856 | bytes 6819840 | tf_op jit(solution)/shard_map/hpq,qhd->phd/dot_general | solution.py:139
  91.9 4.7 %all_to_all.25 = bf16[2,128,2048]{2,1,0:T(8,128)(2,1)S(1)} all-to-all(bf16[2,128,2048]{2,1,0:T(8,128)(2,1)S(1)} %bitcast.94), channel_id=1, replica_groups=mesh['sp'=64,'tp'=2] {'tp'}, dimensions={0} | all-to-all | bytes 2097152 | tf_op jit(solution)/shard_map/all_to_all | solution.py:33
  98.4 48.1 %all_to_all.26 = bf16[64,8,2048]{2,1,0:T(8,128)(2,1)S(1)} all-to-all(bf16[64,8,2048]{2,1,0:T(8,128)(2,1)S(1)} %fusion.15), channel_id=1, replica_groups=mesh['sp'=64,'tp'=2] {'sp'}, dimensions={0} | all-to-all | bytes 4194304 | tf_op jit(solution)/shard_map/all_to_all | solution.py:165
  147.0 7.4 %all_to_all.27 = bf16[2,64,1,8,2048]{4,3,1,2,0:T(8,128)(2,1)S(1)} all-to-all(bf16[2,64,1,8,2048]{4,3,1,2,0:T(8,128)(2,1)S(1)} %broadcast_in_dim.24), channel_id=1, replica_groups=mesh['sp'=64,'tp'=2] {'tp'}, dimensions={0} | all-to-all | bytes 8388608 | tf_op jit(solution)/shard_map/all_to_all | solution.py:39
  155.0 2.1 copy-done.4
  157.1 9.8 %fusion.5 = f32[1024,1792]{1,0:T(8,128)} fusion(bf16[1024,2048]{1,0:T(8,128)(2,1)S(1)} %bitcast.91, bf16[1,2048,1792]{2,1,0:T(8,128)(2,1)S(1)} %bitcast.101), kind=kOutput, calls=%fused_computation.6 | convolution fusion | flops 7516192768 | bytes 18874368 | tf_op jit(solution)/shard_map/dot_general | solution.py:168
  167.0 25.8 %fusion.12 = bf16[1024,2048]{1,0:T(8,128)(2,1)} fusion(bf16[1,1792,2048]{2,1,0:T(8,128)(2,1)} %param.30, f32[1024,1792]{1,0:T(8,128)} %fusion.5, bf16[1024,2048]{1,0:T(8,128)(2,1)} %bitcast.92, bf16[1,2048,1792]{2,1,0:T(8,128)(2,1)} %param.29), kind=kOutput, calls=%fused_computation.16 | convolution fusion | flops 15045492736 | bytes 30408704 | tf_op jit(solution)/shard_map/dot_general | solution.py:171
  192.8 2.5 copy.79
  195.3 8.2 %all_to_all.28 = bf16[2,64,1,8,2048]{4,3,1,2,0:T(8,128)(2,1)} all-to-all(bf16[2,64,1,8,2048]{4,3,1,2,0:T(8,128)(2,1)S(1)} %bitcast.89), channel_id=1, replica_groups=mesh['sp'=64,'tp'=2] {'tp'}, dimensions={0} | all-to-all | bytes 8388608 | tf_op jit(solution)/shard_map/all_to_all | solution.py:33
  203.5 5.1 %reduce_sum.104 = bf16[64,8,2048]{2,1,0:T(8,128)(2,1)} reduce(bf16[2,64,1,8,2048]{4,3,1,2,0:T(8,128)(2,1)} %all_to_all.28, bf16[]{:T(256)} %constant.67.clone.1), dimensions={0,2}, to_apply=%region_9.10 | reduce | flops 1048576 | bytes 6291458 | tf_op jit(solution)/shard_map/reduce_sum | solution.py:34
  208.6 9.9 %all-to-all-start.4 = ((bf16[64,8,2048]{2,1,0:T(8,128)(2,1)}), bf16[64,8,2048]{2,1,0:T(8,128)(2,1)}, u32[]{:S(2)}, u32[]{:S(2)}) async-start(bf16[64,8,2048]{2,1,0:T(8,128)(2,1)} %reduce_sum.104), calls=%async_computation.4 | async-start | bytes 4194304 | tf_op jit(solution)/shard_map/all_to_all | solution.py:178
  219.0 25.8 %all-to-all-done.4 = bf16[64,8,2048]{2,1,0:T(8,128)(2,1)} async-done(((bf16[64,8,2048]{2,1,0:T(8,128)(2,1)}), bf16[64,8,2048]{2,1,0:T(8,128)(2,1)}, u32[]{:S(2)}, u32[]{:S(2)}) %all-to-all-start.4) | async-done | bytes 2097184 | tf_op jit(solution)/shard_map/all_to_all | solution.py:178
  244.8 5.4 %gather_fusion = bf16[256,2048]{1,0:T(8,128)(2,1)} fusion(bf16[512,2048]{1,0:T(8,128)(2,1)} %bitcast.19, s32[1024]{0:T(1024)S(1)} %pad_clamp_fusion), kind=kCustom, calls=%fused_computation | custom fusion | bytes 2098176 | tf_op jit(solution)/shard_map/jit(_take)/gather | solution.py:187
  250.2 2.6 gather.7
  252.7 5.5 %multiply_reduce_fusion = f32[128,2048]{1,0:T(8,128)S(1)} fusion(bf16[128,2,2048]{2,1,0:T(2,128)(2,1)} %gather.7, pred[128,2]{1,0:T(8,128)(4,1)S(1)} %copy.64, f32[128,2]{1,0:T(8,128)S(1)} %copy.68), kind=kLoop, calls=%fused_computation.23 | loop fusion | flops 1835008 | bytes 2098432 | tf_op jit(solution)/shard_map/reduce_sum | solution.py:191
  (103 shorter events, 25.1 us)
Async XLA Ops:
  0.0 90.2 %copy-start = (bf16[512,2048]{1,0:T(8,128)(2,1)S(1)}, bf16[512,2048]{1,0:T(8,128)(2,1)}, u32[]{:S(2)}) copy-start(bf16[512,2048]{1,0:T(8,128)(2,1)} %param.23) | copy-start | bytes 6291460
  0.0 78.1 %copy-start.6 = (bf16[256,512]{1,0:T(8,128)(2,1)S(1)}, bf16[256,512]{1,0:T(8,128)(2,1)}, u32[]{:S(2)}) copy-start(bf16[256,512]{1,0:T(8,128)(2,1)} %param.19) | copy-start | bytes 786436
  0.0 75.5 %collective-permute-start = (bf16[256,256]{1,0:T(8,128)(2,1)}, bf16[256,256]{1,0:T(8,128)(2,1)S(1)}, u32[]{:S(2)}, u32[]{:S(2)}) collective-permute-start(bf16[256,256]{1,0:T(8,128)(2,1)} %param.16), channel_id=1, source_target_pairs={{0,8},{2,10},{4,12},{6,14},{8,16},{10,18},{12,20},{14,22},{16,24},... | collective-permute-start | bytes 393224 | tf_op jit(solution)/shard_map/ppermute | solution.py:22
  3.6 72.0 %collective-permute-start.1 = (bf16[256,256]{1,0:T(8,128)(2,1)}, bf16[256,256]{1,0:T(8,128)(2,1)S(1)}, u32[]{:S(2)}, u32[]{:S(2)}) collective-permute-start(bf16[256,256]{1,0:T(8,128)(2,1)} %param.16), channel_id=1, source_target_pairs={{0,6},{2,8},{4,10},{6,12},{8,14},{10,16},{12,18},{14,20},{16,22},{... | collective-permute-start | bytes 393224 | tf_op jit(solution)/shard_map/ppermute | solution.py:22
  6.8 68.8 %collective-permute-start.2 = (bf16[256,256]{1,0:T(8,128)(2,1)}, bf16[256,256]{1,0:T(8,128)(2,1)S(1)}, u32[]{:S(2)}, u32[]{:S(2)}) collective-permute-start(bf16[256,256]{1,0:T(8,128)(2,1)} %param.16), channel_id=1, source_target_pairs={{0,4},{2,6},{4,8},{6,10},{8,12},{10,14},{12,16},{14,18},{16,20},{1... | collective-permute-start | bytes 393224 | tf_op jit(solution)/shard_map/ppermute | solution.py:22
  11.4 64.2 %collective-permute-start.3 = (bf16[256,256]{1,0:T(8,128)(2,1)}, bf16[256,256]{1,0:T(8,128)(2,1)S(1)}, u32[]{:S(2)}, u32[]{:S(2)}) collective-permute-start(bf16[256,256]{1,0:T(8,128)(2,1)} %param.16), channel_id=1, source_target_pairs={{0,2},{2,4},{4,6},{6,8},{8,10},{10,12},{12,14},{14,16},{16,18},{18... | collective-permute-start | bytes 393224 | tf_op jit(solution)/shard_map/ppermute | solution.py:22
  14.2 8.6 %collective-permute-start.4 = (s32[256]{0:T(256)}, s32[256]{0:T(256)S(1)}, u32[]{:S(2)}, u32[]{:S(2)}) collective-permute-start(s32[256]{0:T(256)} %param.18), channel_id=1, source_target_pairs={{0,8},{2,10},{4,12},{6,14},{8,16},{10,18},{12,20},{14,22},{16,24},... | collective-permute-start | bytes 3080 | tf_op jit(solution)/shard_map/ppermute | solution.py:22
  22.8 6.6 %collective-permute-start.5 = (s32[256]{0:T(256)}, s32[256]{0:T(256)S(1)}, u32[]{:S(2)}, u32[]{:S(2)}) collective-permute-start(s32[256]{0:T(256)} %param.18), channel_id=1, source_target_pairs={{0,6},{2,8},{4,10},{6,12},{8,14},{10,16},{12,18},{14,20},{16,22},{... | collective-permute-start | bytes 3080 | tf_op jit(solution)/shard_map/ppermute | solution.py:22
  29.4 7.2 %collective-permute-start.6 = (s32[256]{0:T(256)}, s32[256]{0:T(256)S(1)}, u32[]{:S(2)}, u32[]{:S(2)}) collective-permute-start(s32[256]{0:T(256)} %param.18), channel_id=1, source_target_pairs={{0,4},{2,6},{4,8},{6,10},{8,12},{10,14},{12,16},{14,18},{16,20},{1... | collective-permute-start | bytes 3080 | tf_op jit(solution)/shard_map/ppermute | solution.py:22
  36.6 5.8 %collective-permute-start.7 = (s32[256]{0:T(256)}, s32[256]{0:T(256)S(1)}, u32[]{:S(2)}, u32[]{:S(2)}) collective-permute-start(s32[256]{0:T(256)} %param.18), channel_id=1, source_target_pairs={{0,2},{2,4},{4,6},{6,8},{8,10},{10,12},{12,14},{14,16},{16,18},{18... | collective-permute-start | bytes 3080 | tf_op jit(solution)/shard_map/ppermute | solution.py:22
  42.4 6.0 %collective-permute-start.8 = (bf16[256,64]{0,1:T(8,128)(2,1)}, bf16[256,64]{0,1:T(8,128)(2,1)S(1)}, u32[]{:S(2)}, u32[]{:S(2)}) collective-permute-start(bf16[256,64]{0,1:T(8,128)(2,1)} %param.17), channel_id=1, source_target_pairs={{0,8},{2,10},{4,12},{6,14},{8,16},{10,18},{12,20},{14,22},{16,24},... | collective-permute-start | bytes 98312 | tf_op jit(solution)/shard_map/ppermute | solution.py:22
  48.4 6.9 %collective-permute-start.9 = (bf16[256,64]{0,1:T(8,128)(2,1)}, bf16[256,64]{0,1:T(8,128)(2,1)S(1)}, u32[]{:S(2)}, u32[]{:S(2)}) collective-permute-start(bf16[256,64]{0,1:T(8,128)(2,1)} %param.17), channel_id=1, source_target_pairs={{0,6},{2,8},{4,10},{6,12},{8,14},{10,16},{12,18},{14,20},{16,22},{... | collective-permute-start | bytes 98312 | tf_op jit(solution)/shard_map/ppermute | solution.py:22
  55.3 9.1 %collective-permute-start.10 = (bf16[256,64]{0,1:T(8,128)(2,1)}, bf16[256,64]{0,1:T(8,128)(2,1)S(1)}, u32[]{:S(2)}, u32[]{:S(2)}) collective-permute-start(bf16[256,64]{0,1:T(8,128)(2,1)} %param.17), channel_id=1, source_target_pairs={{0,4},{2,6},{4,8},{6,10},{8,12},{10,14},{12,16},{14,18},{16,20},{1... | collective-permute-start | bytes 98312 | tf_op jit(solution)/shard_map/ppermute | solution.py:22
  64.4 9.7 %collective-permute-start.11 = (bf16[256,64]{0,1:T(8,128)(2,1)}, bf16[256,64]{0,1:T(8,128)(2,1)S(1)}, u32[]{:S(2)}, u32[]{:S(2)}) collective-permute-start(bf16[256,64]{0,1:T(8,128)(2,1)} %param.17), channel_id=1, source_target_pairs={{0,2},{2,4},{4,6},{6,8},{8,10},{10,12},{12,14},{14,16},{16,18},{18... | collective-permute-start | bytes 98312 | tf_op jit(solution)/shard_map/ppermute | solution.py:22
  80.0 2.3 copy-start.2
  82.4 1.0 copy-start.7
  90.2 6.7 %copy-start.3 = (bf16[128,2048]{1,0:T(8,128)(2,1)S(1)}, bf16[128,2048]{1,0:T(8,128)(2,1)}, u32[]{:S(2)}) copy-start(bf16[128,2048]{1,0:T(8,128)(2,1)} %param.24) | copy-start | bytes 1572868
  90.2 7.2 %copy-start.9 = (f32[2048]{0:T(1024)S(1)}, f32[2048]{0:T(1024)}, u32[]{:S(2)}) copy-start(f32[2048]{0:T(1024)} %param.25) | copy-start | bytes 24580
  91.9 5.7 %copy-start.5 = (s32[512,128]{1,0:T(8,128)S(1)}, s32[512,128]{1,0:T(8,128)}, u32[]{:S(2)}) copy-start(s32[512,128]{1,0:T(8,128)} %convert_reduce_fusion.1) | copy-start | bytes 786436
  147.0 10.1 %slice-start = ((s8[7340032]{0:T(1024)(128)(4,1)}), s8[4194304]{0:T(1024)(128)(4,1)S(1)}, s32[]{:S(2)}) async-start(s8[7340032]{0:T(1024)(128)(4,1)} %bitcast.100), calls=%async_computation.5 | async-start | bytes 8388608
  154.4 2.7 %slice-start.1 = ((s8[7340032]{0:T(1024)(128)(4,1)}), s8[3145728]{0:T(1024)(128)(4,1)S(1)}, s32[]{:S(2)}) async-start(s8[7340032]{0:T(1024)(128)(4,1)} %bitcast.100), calls=%async_computation.6 | async-start | bytes 6291456
  155.0 2.1 copy-start.4
  203.5 15.0 %copy-start.8 = (s32[128,2]{0,1:T(2,128)S(1)}, s32[128,2]{0,1:T(2,128)}, u32[]{:S(2)}) copy-start(s32[128,2]{0,1:T(2,128)} %param.26) | copy-start | bytes 3076
  203.5 15.4 %copy-start.11 = (f32[128,2]{0,1:T(2,128)S(1)}, f32[128,2]{0,1:T(2,128)}, u32[]{:S(2)}) copy-start(f32[128,2]{0,1:T(2,128)} %param.27) | copy-start | bytes 3076
  208.6 36.3 %all-to-all-start.4 = ((bf16[64,8,2048]{2,1,0:T(8,128)(2,1)}), bf16[64,8,2048]{2,1,0:T(8,128)(2,1)}, u32[]{:S(2)}, u32[]{:S(2)}) async-start(bf16[64,8,2048]{2,1,0:T(8,128)(2,1)} %reduce_sum.104), calls=%async_computation.4 | async-start | bytes 4194304 | tf_op jit(solution)/shard_map/all_to_all | solution.py:178
  244.8 15.0 %copy-start.1 = (bf16[512,2048]{1,0:T(8,128)(2,1)S(1)}, bf16[512,2048]{1,0:T(8,128)(2,1)}, u32[]{:S(2)}) copy-start(bf16[512,2048]{1,0:T(8,128)(2,1)} %param.23) | copy-start | bytes 6291460
  250.2 8.6 %copy-start.10 = (f32[2048]{0:T(1024)S(1)}, f32[2048]{0:T(1024)}, u32[]{:S(2)}) copy-start(f32[2048]{0:T(1024)} %param.31) | copy-start | bytes 24580
where the time goes:
time: 265 us; the launch traced here: 260 us
  blocking collectives  68.4 us (26%)
  starting transfers between devices  63.1 us (24%)
  matrix products  48.3 us (18%)
  waiting for transfers between devices  39 us (15%)
  local copies, waits for them, and re-layouts  21.4 us (8%)
  other arithmetic  19.2 us (7%)
    ppermute x12, starting transfers between devices, shifted(): lax.ppermute(value, axis, [(source, source + steps) for source in range(l...  53.2 us
    all_to_all x1, blocking collectives, per_device(): lax.all_to_all(outbound, 'sp', split_axis=0, concat_axis=0, tiled=True)  48.1 us
    dot_general x1, matrix products, per_device(): jnp.dot(hidden, w_down[0], preferred_element_type=jnp.float32)  25.8 us
    all_to_all x1, waiting for transfers between devices, per_device(): lax.all_to_all(reduced.reshape(chip_count, capacity, model_width), 'sp',...  25.8 us
    ppermute x12, waiting for transfers between devices, shifted(): lax.ppermute(value, axis, [(source, source + steps) for source in range(l...  13.2 us
    all_to_all x2, blocking collectives, sum_at_owner(): tiles = lax.all_to_all(in_blocks(x, dim, peers), axis, 0, 0, tiled=True)  12.9 us
    all_to_all x1, starting transfers between devices, per_device(): lax.all_to_all(reduced.reshape(chip_count, capacity, model_width), 'sp',...  9.91 us
    dot_general x1, matrix products, per_device(): gate_pre = jnp.dot(flat_rows, w_gate[0], preferred_element_type=jnp.float32)  9.84 us
  transfers between devices with their start and end apart: 13, of which 8 were waited for; matrix products, arithmetic and copies ran while one was open for 4% of the time, Pallas kernels for 0%

commit v1 on v0

v1 whole, which is shorter than its diff:
```python
import functools

import jax
import jax.numpy as jnp
from jax import lax
from jax.experimental import pallas as pl
from jax.experimental.pallas import tpu as pltpu
from jax.sharding import PartitionSpec as P

HEADS = 8
DK = 128
DR = 64
DV = 128
TOPK = 2
REACH = 4
RANK = 256
D = 2048
TOK = 256
ROWS = 128
FFH = 1792
CAP = 8
GROUPS = 4
PEERS = 16
LOCAL_HEADS = 4
CHIPS = 64

ROPE_THETA = 500000.0
RESIDUAL_SCALE = 2.0**0.5
NORM_EPSILON = 1e-05
EXCLUDED = -1e30
MESH = pl.DeviceIdType.MESH
VMEM_LIMIT = 67_000_000
F32 = jnp.float32
BF16 = jnp.bfloat16


def remote(src, dst, send, recv, chip, core):
    return pltpu.make_async_remote_copy(
        src_ref=src, dst_ref=dst, send_sem=send, recv_sem=recv, device_id=(chip, core), device_id_type=MESH
    )


def layer_norm(values, gain_vec):
    centre = jnp.mean(values, -1, keepdims=True)
    spread = jnp.mean(jnp.square(values - centre), -1, keepdims=True)
    return (values - centre) * lax.rsqrt(spread + NORM_EPSILON) * gain_vec


def attention_kernel(
    msg,
    qc,
    qaux,
    wk_hbm,
    wv_hbm,
    wo_hbm,
    residual,
    gain,
    out,
    kv,
    wk,
    wv,
    wo,
    scores,
    vals,
    att,
    psend,
    precv,
    wsem,
    ssem,
    rsem,
    fssem,
    frsem,
    psem,
):
    sp = lax.axis_index("sp")
    tp = lax.axis_index("tp")
    other = 1 - tp
    half = LOCAL_HEADS * DK
    cols = pl.ds(pl.multiple_of(tp * half, half), half)
    loads = [
        pltpu.make_async_copy(wk_hbm.at[:, cols], wk, wsem.at[0]),
        pltpu.make_async_copy(wv_hbm.at[:, cols], wv, wsem.at[1]),
        pltpu.make_async_copy(wo_hbm, wo, wsem.at[2]),
    ]
    for load in loads:
        load.start()
    barrier = pltpu.get_barrier_semaphore()
    for step in (1, 2, 3, 4, -1, -2, -3, -4):
        pl.semaphore_signal(
            barrier, inc=1, device_id=(lax.rem(sp + step + CHIPS, CHIPS), tp), device_id_type=MESH
        )
    pl.semaphore_signal(barrier, inc=1, device_id=(sp, other), device_id_type=MESH)
    pl.semaphore_wait(barrier, 2 * REACH + 1)

    mine = pl.ds(pl.multiple_of(tp * ROWS, ROWS), ROWS)
    sends = []
    for d in range(1, REACH + 1):
        sends.append(
            remote(
                msg.at[mine],
                kv.at[d - 1, tp],
                ssem.at[d - 1],
                rsem.at[d - 1],
                lax.rem(sp + d, CHIPS),
                tp,
            )
        )
        sends[-1].start()
    loads[0].wait()
    loads[1].wait()

    def block(rows, slot, causal):
        lat = rows[:, :RANK]
        aux = rows[:, RANK:]
        keys = jnp.dot(lat, wk[...], preferred_element_type=F32).astype(BF16)
        vals[pl.ds(slot * TOK, TOK), :] = jnp.dot(lat, wv[...], preferred_element_type=F32).astype(BF16)
        for h in range(LOCAL_HEADS):
            hs = slice(h * DK, (h + 1) * DK)
            query = jnp.concatenate([qc[:, hs], qaux[:, hs]], 1)
            key = jnp.concatenate([keys[:, hs], aux], 1)
            s = lax.dot_general(query, key, (((1,), (1,)), ((), ())), preferred_element_type=F32)
            if causal:
                r = lax.broadcasted_iota(jnp.int32, (TOK, TOK), 0)
                c = lax.broadcasted_iota(jnp.int32, (TOK, TOK), 1)
                s = jnp.where(c <= r, s, EXCLUDED)
            scores[h, :, slot * TOK : (slot + 1) * TOK] = s

    block(msg[...], 0, True)
    forwards = []
    for d in range(REACH):
        sends[d].wait_recv()
        forwards.append(remote(kv.at[d, tp], kv.at[d, tp], fssem.at[d], frsem.at[d], sp, other))
        forwards[-1].start()
        if d >= 1:
            remote(kv.at[d - 1, other], kv.at[d - 1, other], fssem.at[d - 1], frsem.at[d - 1], sp, other).wait_recv()
            block(kv[d - 1].reshape(TOK, RANK + 128), d, False)
    last = REACH - 1
    remote(kv.at[last, other], kv.at[last, other], fssem.at[last], frsem.at[last], sp, other).wait_recv()
    block(kv[last].reshape(TOK, RANK + 128), REACH, False)

    scale = (DK + DR) ** (-0.5)
    for h in range(LOCAL_HEADS):
        s = scores[h]
        peak = jnp.max(s, -1, keepdims=True)
        lifted = jnp.exp((s - peak) * scale)
        total = jnp.sum(lifted, -1, keepdims=True)
        hs = slice(h * DV, (h + 1) * DV)
        mixed = jnp.dot(lifted.astype(BF16), vals[:, hs], preferred_element_type=F32)
        att[:, hs] = (mixed / total).astype(BF16)
    loads[2].wait()
    theirs = pl.ds(pl.multiple_of(other * ROWS, ROWS), ROWS)
    psend[...] = jnp.dot(att[theirs, :], wo[...], preferred_element_type=F32).astype(BF16)
    swap = remote(psend, precv, psem.at[0], psem.at[1], sp, other)
    swap.start()
    own = jnp.dot(att[mine, :], wo[...], preferred_element_type=F32).astype(BF16).astype(F32)
    own = own + RESIDUAL_SCALE * residual[...].astype(F32)
    swap.wait_recv()
    out[...] = layer_norm(own + precv[...].astype(F32), gain[...]).astype(BF16)
    swap.wait_send()
    for d in range(REACH):
        sends[d].wait_send()
        forwards[d].wait_send()


def expert_kernel(
    normed,
    routes,
    weights,
    wg_hbm,
    wu_hbm,
    wd_hbm,
    gain,
    out,
    wg,
    wu,
    wd,
    obuf,
    xbuf,
    hid,
    ykeep,
    ysend,
    yrecv,
    ret,
    back,
    wsem,
    dsend,
    drecv,
    fsend,
    frecv,
    ysendsem,
    yrecvsem,
    bsend,
    brecv,
):
    sp = lax.axis_index("sp")
    tp = lax.axis_index("tp")
    other = 1 - tp
    loads = [
        pltpu.make_async_copy(wg_hbm.at[0], wg, wsem.at[0]),
        pltpu.make_async_copy(wu_hbm.at[0], wu, wsem.at[1]),
        pltpu.make_async_copy(wd_hbm.at[0], wd, wsem.at[2]),
    ]
    for load in loads:
        load.start()
    barrier = pltpu.get_barrier_semaphore()

    def greet(i, carry):
        pl.semaphore_signal(barrier, inc=1, device_id=(lax.rem(sp + i, CHIPS), tp), device_id_type=MESH)
        return carry

    lax.fori_loop(1, CHIPS, greet, 0)
    pl.semaphore_signal(barrier, inc=1, device_id=(sp, other), device_id_type=MESH)

    z, y, x = sp // 16, lax.rem(sp // 4, 4), lax.rem(sp, 4)
    lane = lax.broadcasted_iota(jnp.int32, (ROWS, 128), 1)
    picks = [routes[:, k : k + 1] for k in range(TOPK)]
    member = ((picks[0] == lane) | (picks[1] == lane)).astype(F32).astype(BF16)
    lower = (lane < lax.broadcasted_iota(jnp.int32, (ROWS, 128), 0)).astype(F32).astype(BF16)
    before = jnp.dot(lower, member, preferred_element_type=F32)
    slot_lane = lax.broadcasted_iota(jnp.int32, (ROWS, CHIPS * CAP), 1)
    gathers = []
    for pick in picks:
        rank = jnp.sum(jnp.where(pick == lane, before, 0.0), 1, keepdims=True).astype(jnp.int32)
        oz = lax.bitwise_and((pick >> 4) - z, 3)
        oy = lax.bitwise_and((pick >> 2) - y, 3)
        ox = lax.bitwise_and(pick - x, 3)
        place = lax.bitwise_and(oz + oy + ox, 3) * PEERS + oz * 4 + oy
        gathers.append((slot_lane == place * CAP + rank).astype(F32))
    placing = jnp.transpose(gathers[0] + gathers[1]).astype(BF16)
    gathers = [g.astype(BF16) for g in gathers]
    rows_in = normed[...]

    def there(g, j, sign):
        oz = j // 4
        oy = lax.rem(j, 4)
        ox = lax.rem(g + 8 - oz - oy, 4)
        dz = lax.rem(z + sign * oz + 4, 4)
        dy = lax.rem(y + sign * oy + 4, 4)
        dx = lax.rem(x + sign * ox + 4, 4)
        return dz * 16 + dy * 4 + dx

    pl.semaphore_wait(barrier, CHIPS)
    for g in range(GROUPS):
        obuf[g] = (
            jnp.dot(placing[g * ROWS : (g + 1) * ROWS], rows_in, preferred_element_type=F32)
            .astype(BF16)
            .reshape(PEERS, CAP, D)
        )
        first = 1 if g == 0 else 0

        def dispatch(j, carry, g=g):
            remote(obuf.at[g, j], xbuf.at[g, tp, j], dsend.at[g], drecv.at[g], there(g, j, 1), tp).start()
            return carry

        lax.fori_loop(first, PEERS, dispatch, 0)
        if g == 0:
            xbuf[0, tp, 0] = obuf[0, 0]

    def arrived(g):
        first = 1 if g == 0 else 0
        part = xbuf.at[g, tp, pl.ds(first, PEERS - first)]
        remote(part, part, dsend.at[g], drecv.at[g], sp, other).wait_recv()
        fwd = remote(xbuf.at[g, tp], xbuf.at[g, tp], fsend.at[g], frecv.at[g], sp, other)
        fwd.start()

    arrived(0)
    for g in range(GROUPS):
        theirs = xbuf.at[g, other]
        remote(theirs, theirs, fsend.at[g], frecv.at[g], sp, other).wait_recv()
        if g == 0:
            loads[0].wait()
            loads[1].wait()
        rows = xbuf.at[g]

        def upward(n, carry):
            cols = pl.ds(pl.multiple_of(n * 256, 256), 256)
            lhs = rows[...].reshape(TOK, D)
            gate = jnp.dot(lhs, wg[:, cols], preferred_element_type=F32)
            up = jnp.dot(lhs, wu[:, cols], preferred_element_type=F32)
            hid[:, cols] = (gate / (1.0 + jnp.exp(-gate)) * up).astype(BF16)
            return carry

        lax.fori_loop(0, FFH // 256, upward, 0)
        if g == 0:
            loads[2].wait()

        def downward(n, carry):
            cols = pl.ds(pl.multiple_of(n * 256, 256), 256)
            ysend[g, :, cols] = jnp.dot(
                hid[pl.ds(pl.multiple_of(other * ROWS, ROWS), ROWS), :], wd[:, cols], preferred_element_type=F32
            ).astype(BF16)
            ykeep[:, cols] = jnp.dot(
                hid[pl.ds(pl.multiple_of(tp * ROWS, ROWS), ROWS), :], wd[:, cols], preferred_element_type=F32
            ).astype(BF16)
            return carry

        lax.fori_loop(0, D // 256, downward, 0)
        swap = remote(ysend.at[g], yrecv.at[g], ysendsem.at[g], yrecvsem.at[g], sp, other)
        swap.start()
        if g + 1 < GROUPS:
            arrived(g + 1)
        swap.wait_recv()
        ret[g] = (ykeep[...].astype(F32) + yrecv[g].astype(F32)).astype(BF16).reshape(PEERS, CAP, D)
        first = 1 if g == 0 else 0

        def send_back(j, carry):
            remote(ret.at[g, j], back.at[g, j], bsend.at[g], brecv.at[g], there(g, j, -1), tp).start()
            return carry

        lax.fori_loop(first, PEERS, send_back, 0)
        if g == 0:
            back[0, 0] = ret[0, 0]

    combined = RESIDUAL_SCALE * normed[...].astype(F32)
    picked = [jnp.zeros((ROWS, D), F32) for _ in range(TOPK)]
    for g in range(GROUPS):
        first = 1 if g == 0 else 0
        part = back.at[g, pl.ds(first, PEERS - first)]
        remote(part, part, bsend.at[g], brecv.at[g], sp, other).wait_recv()
        landed = back[g].reshape(ROWS, D)
        for k in range(TOPK):
            picked[k] = picked[k] + jnp.dot(
                gathers[k][:, g * ROWS : (g + 1) * ROWS], landed, preferred_element_type=F32
            )
    for k in range(TOPK):
        combined = combined + picked[k] * weights[:, k : k + 1]
    out[...] = layer_norm(combined, gain[...]).astype(BF16)
    for g in range(GROUPS):
        first = 1 if g == 0 else 0
        part = obuf.at[g, pl.ds(first, PEERS - first)]
        remote(part, part, dsend.at[g], drecv.at[g], sp, other).wait_send()
        part = ret.at[g, pl.ds(first, PEERS - first)]
        remote(part, part, bsend.at[g], brecv.at[g], sp, other).wait_send()
        remote(xbuf.at[g, tp], xbuf.at[g, tp], fsend.at[g], frecv.at[g], sp, other).wait_send()
        remote(ysend.at[g], ysend.at[g], ysendsem.at[g], yrecvsem.at[g], sp, other).wait_send()


def in_vmem():
    return pl.BlockSpec(memory_space=pltpu.VMEM)


def in_hbm():
    return pl.BlockSpec(memory_space=pl.ANY)


DMA = pltpu.SemaphoreType.DMA


def attend(msg, qc, qaux, w_key_up, w_value_up, w_out, residual, gain):
    return pl.pallas_call(
        attention_kernel,
        out_shape=jax.ShapeDtypeStruct((ROWS, D), BF16),
        in_specs=[in_vmem()] * 3 + [in_hbm()] * 3 + [in_vmem()] * 2,
        out_specs=in_vmem(),
        scratch_shapes=[
            pltpu.VMEM((REACH, 2, ROWS, RANK + 128), BF16),
            pltpu.VMEM((RANK, LOCAL_HEADS * DK), BF16),
            pltpu.VMEM((RANK, LOCAL_HEADS * DV), BF16),
            pltpu.VMEM((LOCAL_HEADS * DV, D), BF16),
            pltpu.VMEM((LOCAL_HEADS, TOK, (REACH + 1) * TOK), F32),
            pltpu.VMEM(((REACH + 1) * TOK, LOCAL_HEADS * DV), BF16),
            pltpu.VMEM((TOK, LOCAL_HEADS * DV), BF16),
            pltpu.VMEM((ROWS, D), BF16),
            pltpu.VMEM((ROWS, D), BF16),
            DMA((3,)),
            DMA((REACH,)),
            DMA((REACH,)),
            DMA((REACH,)),
            DMA((REACH,)),
            DMA((2,)),
        ],
        compiler_params=pltpu.CompilerParams(
            collective_id=0, has_side_effects=True, vmem_limit_bytes=VMEM_LIMIT
        ),
    )(msg, qc, qaux, w_key_up, w_value_up, w_out, residual, gain)


def route_and_mix(normed, routes, route_weights, w_gate, w_up, w_down, gain):
    return pl.pallas_call(
        expert_kernel,
        out_shape=jax.ShapeDtypeStruct((ROWS, D), BF16),
        in_specs=[in_vmem()] * 3 + [in_hbm()] * 3 + [in_vmem()],
        out_specs=in_vmem(),
        scratch_shapes=[
            pltpu.VMEM((D, FFH), BF16),
            pltpu.VMEM((D, FFH), BF16),
            pltpu.VMEM((FFH, D), BF16),
            pltpu.VMEM((GROUPS, PEERS, CAP, D), BF16),
            pltpu.VMEM((GROUPS, 2, PEERS, CAP, D), BF16),
            pltpu.VMEM((TOK, FFH), BF16),
            pltpu.VMEM((ROWS, D), BF16),
            pltpu.VMEM((GROUPS, ROWS, D), BF16),
            pltpu.VMEM((GROUPS, ROWS, D), BF16),
            pltpu.VMEM((GROUPS, PEERS, CAP, D), BF16),
            pltpu.VMEM((GROUPS, PEERS, CAP, D), BF16),
            DMA((3,)),
        ]
        + [DMA((GROUPS,))] * 8,
        compiler_params=pltpu.CompilerParams(
            collective_id=1, has_side_effects=True, vmem_limit_bytes=VMEM_LIMIT
        ),
    )(normed, routes, route_weights, w_gate, w_up, w_down, gain)


def rotate(values, positions):
    half_width = values.shape[-1] // 2
    frequency = ROPE_THETA ** (-2.0 * jnp.arange(half_width, dtype=jnp.float32) / values.shape[-1])
    angles = positions.astype(jnp.float32)[:, None] * frequency[None, :]
    table_shape = (values.shape[0],) + (1,) * (values.ndim - 2) + (half_width,)
    cosine = jnp.cos(angles).reshape(table_shape)
    sine_part = jnp.sin(angles).reshape(table_shape)
    widened = values.astype(jnp.float32)
    first_half = widened[..., :half_width]
    second = widened[..., half_width:]
    return jnp.concatenate(
        [first_half * cosine - second * sine_part, second * cosine + first_half * sine_part], -1
    )


def per_device(
    latent,
    rotary_key,
    doc_ids,
    queries_content,
    queries_rotary,
    w_key_up,
    w_value_up,
    w_out,
    residual,
    norm_gain,
    routes,
    route_weights,
    w_gate,
    w_up,
    w_down,
    out_gain,
):
    sp_index = lax.axis_index("sp")
    own_position = sp_index * TOK + jnp.arange(TOK, dtype=jnp.int32)
    query_turned = rotate(queries_rotary.reshape(TOK, LOCAL_HEADS, DR), own_position).astype(BF16)
    key_turned = rotate(rotary_key, own_position).astype(BF16)
    doc = jnp.arange(64, dtype=jnp.int32)[None, :]
    same = doc == doc_ids[:, None]
    marks = same.astype(BF16)
    fence = jnp.where(same | (doc >= 32), 0.0, EXCLUDED).astype(BF16)
    msg = jnp.concatenate([latent, key_turned, marks], 1)
    fences = jnp.broadcast_to(fence[:, None, :], (TOK, LOCAL_HEADS, 64))
    qaux = jnp.concatenate([query_turned, fences], -1).reshape(TOK, LOCAL_HEADS * 128)
    normed = attend(
        msg, queries_content, qaux, w_key_up, w_value_up, w_out, residual, norm_gain.reshape(1, D)
    )
    return route_and_mix(normed, routes, route_weights, w_gate, w_up, w_down, out_gain.reshape(1, D))


def solution(mesh):
    return jax.shard_map(
        per_device,
        mesh=mesh,
        in_specs=(
            P("sp", None),
            P("sp", None),
            P("sp"),
            P("sp", "tp"),
            P("sp", "tp"),
            P(),
            P(),
            P("tp", None),
            P(("sp", "tp"), None),
            P(),
            P(("sp", "tp"), None),
            P(("sp", "tp"), None),
            P("sp", None, "tp"),
            P("sp", None, "tp"),
            P("sp", "tp", None),
            P(),
        ),
        out_specs=P(("sp", "tp"), None),
        check_vma=False,
    )
```

time: 265 us -> 113 us (0.43)
  the two profiles are of different devices: /device:TPU:12 before, /device:TPU:1 now
where the time goes in v1:
time: 113 us
  Pallas kernels  102 us (90%)
  local copies, waits for them, and re-layouts  6.58 us (6%)
  other arithmetic  4.5 us (4%)
    pallas_call x1, Pallas kernels, route_and_mix(): pl.pallas_call(expert_kernel, out_shape=jax.ShapeDtypeStruct((ROWS, D), B...  74.4 us
    pallas_call x1, Pallas kernels, attend(): pl.pallas_call(attention_kernel, out_shape=jax.ShapeDtypeStruct((ROWS, D)...  27.5 us
    unnamed x10, local copies, waits for them, and re-layouts  6.01 us

profile of v1, /device:TPU:1, one launch (start us, length us, event | category | flops | bytes accessed | tf_op | source)
XLA Modules:
  0.0 113.0 jit_solution(13542568108470245529)
XLA Ops:
  0.0 0.0 copy-start
  0.0 0.0 copy-start.1
  0.0 0.9 copy.28
  1.0 0.6 multiply_cosine_fusion
  1.5 0.1 copy.31
  1.6 0.1 copy.32
  1.7 1.0 copy.30
  2.8 0.2 copy.33
  3.0 0.2 copy.34
  3.2 0.8 select_convert_fusion
  3.9 0.1 broadcast_in_dim.12
  4.0 0.6 pad_maximum_fusion
  4.6 0.7 copy.39
  5.4 0.8 fusion.1
  6.1 1.7 %pad_maximum_fusion.1.msg = bf16[256,384]{1,0:T(8,128)(2,1)} fusion(bf16[256,64]{1,0:T(8,128)(2,1)S(1)} %fusion.1, bf16[256,32]{1,0:T(8,128)(2,1)S(1)} %get-tuple-element.11, bf16[256,32]{1,0:T(8,128)(2,1)S(1)} %get-tuple-element.12, bf16[256,256]{1,0:T(8,128)(2,1)} %param.16), kind=kLoop, calls=%fused_computation.2 | loop fusion | flops 786432 | bytes 393216 | tf_op jit(solution)/shard_map/concatenate | solution.py:446
  7.8 27.5 %shard_map.154.normed = bf16[128,2048]{1,0:T(8,128)(2,1)} custom-call(bf16[256,384]{1,0:T(8,128)(2,1)} %pad_maximum_fusion.1.msg, bf16[256,512]{1,0:T(8,128)(2,1)} %qc.1, bf16[256,512]{1,0:T(8,128)(2,1)} %bitcast.8, bf16[256,1024]{1,0:T(8,128)(2,1)} %wk_hbm.1, bf16[256,1024]{1,0:T(8,128)(2,1)} %wv_hbm.1, bf16[512,2048]{1,0:T(8,128)(2,1)} %wo_hbm.1, ...), custom_call_target="tpu_custom_call" | custom-call | tf_op jit(solution)/shard_map/pallas_call | solution.py:350
  35.3 0.0 copy-done
  35.3 0.7 copy.35.routes
  36.1 0.0 copy-done.1
  36.1 0.7 copy.36.weights
  36.8 74.4 %shard_map.155 = bf16[128,2048]{1,0:T(8,128)(2,1)} custom-call(bf16[128,2048]{1,0:T(8,128)(2,1)} %shard_map.154.normed, s32[128,2]{1,0:T(8,128)} %copy.35.routes, f32[128,2]{1,0:T(8,128)} %copy.36.weights, bf16[1,2048,1792]{2,1,0:T(8,128)(2,1)} %wg_hbm.1, bf16[1,2048,1792]{2,1,0:T(8,128)(2,1)} %wu_hbm.1, bf16[1,1792,2048]{2,1,0:T(8,128)(2,1)} %wd_hbm.1, ...), custom_call_target="tpu_custom_call" | custom-call | tf_op jit(solution)/shard_map/pallas_call | solution.py:379
  111.2 1.9 %copy.41 = bf16[128,2048]{1,0:T(8,128)(2,1)} copy(bf16[128,2048]{1,0:T(8,128)(2,1)} %shard_map.155) | data formatting | bytes 1048576
  (6 shorter events, 0.1 us)
Async XLA Ops:
  0.0 35.3 %copy-start = (s32[128,2]{0,1:T(2,128)S(1)}, s32[128,2]{0,1:T(2,128)}, u32[]{:S(2)}) copy-start(s32[128,2]{0,1:T(2,128)} %param.26) | copy-start | bytes 3076
  0.0 36.1 %copy-start.1 = (f32[128,2]{0,1:T(2,128)S(1)}, f32[128,2]{0,1:T(2,128)}, u32[]{:S(2)}) copy-start(f32[128,2]{0,1:T(2,128)} %param.27) | copy-start | bytes 3076

commit v2 on v1

v2 whole, which is shorter than its diff:
```python
import jax
import jax.numpy as jnp
import numpy as np
from jax import lax
from jax.experimental import pallas as pl
from jax.experimental.pallas import tpu as pltpu
from jax.sharding import PartitionSpec as P

HEADS = 8
DK = 128
DR = 64
DV = 128
TOPK = 2
REACH = 4
RANK = 256
D = 2048
TOK = 256
ROWS = 128
FFH = 1792
CAP = 8
GROUPS = 4
PEERS = 16
LOCAL_HEADS = 4
CHIPS = 64

ROPE_THETA = 500000.0
RESIDUAL_SCALE = 2.0**0.5
NORM_EPSILON = 1e-05
EXCLUDED = -1e30
LOG2E = 1.4426950408889634
MESH = pl.DeviceIdType.MESH
VMEM_LIMIT = 62_000_000
F32 = jnp.float32
BF16 = jnp.bfloat16


def remote(src, dst, send, recv, chip, core):
    return pltpu.make_async_remote_copy(
        src_ref=src, dst_ref=dst, send_sem=send, recv_sem=recv, device_id=(chip, core), device_id_type=MESH
    )


def layer_norm(values, gain_vec):
    centre = jnp.mean(values, -1, keepdims=True)
    spread = jnp.mean(jnp.square(values - centre), -1, keepdims=True)
    return (values - centre) * lax.rsqrt(spread + NORM_EPSILON) * gain_vec


def layer_kernel(
    latent,
    key_rot,
    doc_row,
    frequency,
    gain,
    routes,
    weights,
    last_gain,
    qc_hbm,
    qr_hbm,
    residual_hbm,
    wk_hbm,
    wv_hbm,
    wo_hbm,
    wg_hbm,
    wu_hbm,
    wd_hbm,
    out,
    qc,
    qr,
    residual,
    aux_out,
    qaux,
    kvl,
    kva,
    wk,
    wv,
    wo,
    peaks,
    sums,
    att,
    psend,
    precv,
    nrm,
    wg,
    wu,
    wd,
    obuf,
    xbuf,
    lhs,
    hid,
    ybuf,
    yrecv,
    back,
    wsem,
    ssem,
    rsem,
    fssem,
    frsem,
    psem,
    met,
    dsend,
    drecv,
    fsend,
    frecv,
    ysendsem,
    yrecvsem,
    bsend,
    brecv,
):
    sp = lax.axis_index("sp")
    tp = lax.axis_index("tp")
    other = 1 - tp
    barrier = pltpu.get_barrier_semaphore()

    def signal(semaphore, chip, core):
        pl.semaphore_signal(semaphore, inc=1, device_id=(chip, core), device_id_type=MESH)

    z, y, x = sp // 16, lax.rem(sp // 4, 4), lax.rem(sp, 4)
    y_ring = [z * 16 + lax.rem(y + e, 4) * 4 + x for e in (1, 2, 3)]
    z_ring = [lax.rem(z + e, 4) * 16 + y * 4 + x for e in (1, 2, 3)]
    x_ring = [z * 16 + y * 4 + lax.rem(x + e, 4) for e in (1, 2, 3)]
    near = [lax.rem(sp + e + CHIPS, CHIPS) for e in (1, 2, 3, 4, -1, -2, -3, -4)]
    for chip in near + x_ring + y_ring + z_ring:
        signal(barrier, chip, tp)
    signal(barrier, sp, other)

    half = LOCAL_HEADS * DK
    cols = pl.ds(pl.multiple_of(tp * half, half), half)
    loads = [
        pltpu.make_async_copy(wk_hbm.at[:, cols], wk, wsem.at[0]),
        pltpu.make_async_copy(wv_hbm.at[:, cols], wv, wsem.at[1]),
        pltpu.make_async_copy(wo_hbm, wo, wsem.at[2]),
        pltpu.make_async_copy(wg_hbm.at[0], wg, wsem.at[3]),
        pltpu.make_async_copy(wu_hbm.at[0], wu, wsem.at[4]),
        pltpu.make_async_copy(wd_hbm.at[0], wd, wsem.at[5]),
        pltpu.make_async_copy(qc_hbm, qc, wsem.at[6]),
        pltpu.make_async_copy(qr_hbm, qr, wsem.at[7]),
        pltpu.make_async_copy(residual_hbm, residual, wsem.at[8]),
    ]
    for k in (0, 1, 6, 7, 2, 8):
        loads[k].start()
    mine = pl.ds(pl.multiple_of(tp * ROWS, ROWS), ROWS)
    theirs = pl.ds(pl.multiple_of(other * ROWS, ROWS), ROWS)
    pl.semaphore_wait(barrier, 18)
    latent_sends = []
    for d in range(REACH):
        chip = lax.rem(sp + d + 1, CHIPS)
        latent_sends.append(remote(latent.at[mine], kvl.at[d, tp], ssem.at[0, d], rsem.at[0, d], chip, tp))
        latent_sends[-1].start()

    doc_lane = lax.broadcasted_iota(jnp.int32, (64, TOK), 0)
    marks = (doc_lane == doc_row[...]).astype(F32)
    natural = jnp.transpose(jnp.concatenate([key_rot[...].astype(F32), marks], 0))
    wide = lax.broadcasted_iota(jnp.int32, (TOK, 128), 1)
    content = wide < DR
    low_half = lax.rem(wide, DR) < DR // 2
    position = (sp * TOK + lax.broadcasted_iota(jnp.int32, (TOK, 128), 0)).astype(F32)
    angles = position * frequency[...]
    cos_table = jnp.cos(angles)
    sin_table = jnp.where(low_half, -jnp.sin(angles), jnp.sin(angles))

    def turned(v):
        swapped = jnp.where(low_half, pltpu.roll(v, 128 - DR // 2, 1), pltpu.roll(v, DR // 2, 1))
        return v * cos_table + swapped * sin_table

    aux_out[...] = jnp.where(content, turned(natural), natural).astype(BF16)
    aux_sends = []
    for d in range(REACH):
        chip = lax.rem(sp + d + 1, CHIPS)
        aux_sends.append(remote(aux_out.at[mine], kva.at[d, tp], ssem.at[1, d], rsem.at[1, d], chip, tp))
        aux_sends[-1].start()
    loads[7].wait()
    fence = jnp.where(wide < DR + 32, (natural - 1.0) * -EXCLUDED, 0.0)
    for pair in range(LOCAL_HEADS // 2):
        two = turned(qr[:, pair * 128 : (pair + 1) * 128].astype(F32))
        first = jnp.where(content, two, fence)
        second = jnp.where(content, pltpu.roll(two, DR, 1), fence)
        qaux[:, pair * 256 : pair * 256 + 128] = first.astype(BF16)
        qaux[:, pair * 256 + 128 : pair * 256 + 256] = second.astype(BF16)

    expert = lax.broadcasted_iota(jnp.int32, (128, ROWS), 0)
    picks = [routes[k : k + 1, :] for k in range(TOPK)]
    member = ((picks[0] == expert) | (picks[1] == expert)).astype(F32).astype(BF16)
    upper = (expert < lax.broadcasted_iota(jnp.int32, (128, ROWS), 1)).astype(F32).astype(BF16)
    before = jnp.dot(member, upper, preferred_element_type=F32)
    slots = []
    for pick in picks:
        rank = jnp.sum(jnp.where(pick == expert, before, 0.0), 0, keepdims=True)
        oz = lax.bitwise_and((pick >> 4) - z, 3)
        oy = lax.bitwise_and((pick >> 2) - y, 3)
        ox = lax.bitwise_and(pick - x, 3)
        place = lax.bitwise_and(oz + oy + ox, 3) * PEERS + oz * 4 + oy
        slots.append(place * CAP + rank.astype(jnp.int32))
    slot_sub = lax.broadcasted_iota(jnp.int32, (CHIPS * CAP, ROWS), 0)
    placing = ((slot_sub == slots[0]) | (slot_sub == slots[1])).astype(F32).astype(BF16)
    table = jnp.where(
        expert == 0,
        slots[0].astype(F32),
        jnp.where(
            expert == 1,
            slots[1].astype(F32),
            jnp.where(expert == 2, weights[0:1, :], jnp.where(expert == 3, weights[1:2, :], 0.0)),
        ),
    )
    by_row = jnp.transpose(table)
    slot_lane = lax.broadcasted_iota(jnp.int32, (ROWS, CHIPS * CAP), 1).astype(F32)
    gathers = [(slot_lane == by_row[:, k : k + 1]).astype(F32).astype(BF16) for k in range(TOPK)]
    shares = [by_row[:, TOPK + k : TOPK + k + 1] for k in range(TOPK)]

    for chip in y_ring:
        signal(met.at[0], chip, tp)
    loads[0].wait()
    loads[1].wait()
    loads[6].wait()
    for load in loads[3:6]:
        load.start()

    rate = (DK + DR) ** (-0.5) * LOG2E
    ones = jnp.ones((TOK, DV), BF16)

    def block(lat, aux, first):
        keys = jnp.dot(lat, wk[...], preferred_element_type=F32).astype(BF16)
        values = jnp.dot(lat, wv[...], preferred_element_type=F32).astype(BF16)
        for h in range(LOCAL_HEADS):
            hs = slice(h * DK, (h + 1) * DK)
            query = jnp.concatenate([qc[:, hs], qaux[:, hs]], 1)
            key = jnp.concatenate([keys[:, hs], aux], 1)
            s = lax.dot_general(query, key, (((1,), (1,)), ((), ())), preferred_element_type=F32)
            if first:
                r = lax.broadcasted_iota(jnp.int32, (TOK, TOK), 0)
                c = lax.broadcasted_iota(jnp.int32, (TOK, TOK), 1)
                s = jnp.where(c <= r, s, EXCLUDED)
            peak = jnp.max(s, -1, keepdims=True)
            if not first:
                was = peaks[h][:, :1]
                peak = jnp.maximum(peak, was)
            lifted = jnp.exp2((s - peak) * rate).astype(BF16)
            made = jnp.dot(lifted, jnp.concatenate([values[:, hs], ones], 1), preferred_element_type=F32)
            if not first:
                made = made + sums[h] * jnp.exp2((was - peak) * rate)
            peaks[h] = jnp.broadcast_to(peak, (TOK, 128))
            sums[h] = made

    block(latent[...], aux_out[...], True)
    pl.semaphore_wait(met.at[0], 3)
    for chip in z_ring:
        signal(met.at[1], chip, tp)

    def relays(d, core):
        return [
            remote(part.at[d, core], part.at[d, core], fssem.at[i, d], frsem.at[i, d], sp, other)
            for i, part in enumerate((kvl, kva))
        ]

    def process(d):
        for relay in relays(d, other):
            relay.wait_recv()
        block(kvl[d].reshape(TOK, RANK), kva[d].reshape(TOK, 128), False)

    for d in range(REACH):
        for send, relay in zip((latent_sends[d], aux_sends[d]), relays(d, tp)):
            send.wait_recv()
            relay.start()
        if d >= 1:
            process(d - 1)
    loads[2].wait()
    loads[8].wait()
    process(REACH - 1)

    for h in range(LOCAL_HEADS):
        att[:, h * DV : (h + 1) * DV] = (sums[h, :, :DV] / sums[h, :, DV:]).astype(BF16)
    psend[...] = jnp.dot(att[theirs, :], wo[...], preferred_element_type=F32).astype(BF16)
    swap = remote(psend, precv, psem.at[0], psem.at[1], sp, other)
    swap.start()
    own = jnp.dot(att[mine, :], wo[...], preferred_element_type=F32).astype(BF16).astype(F32)
    own = own + RESIDUAL_SCALE * residual[...].astype(F32)
    swap.wait_recv()
    rows_in = layer_norm(own + precv[...].astype(F32), gain[...]).astype(BF16)
    nrm[...] = rows_in

    def there(g, j, sign):
        oz = j // 4
        oy = lax.rem(j, 4)
        ox = lax.rem(g + 8 - oz - oy, 4)
        dz = lax.rem(z + sign * oz + 4, 4)
        dy = lax.rem(y + sign * oy + 4, 4)
        dx = lax.rem(x + sign * ox + 4, 4)
        return dz * 16 + dy * 4 + dx

    pl.semaphore_wait(met.at[1], 3)
    for g in range(GROUPS):
        obuf[g] = (
            jnp.dot(placing[g * ROWS : (g + 1) * ROWS], rows_in, preferred_element_type=F32)
            .astype(BF16)
            .reshape(PEERS, CAP, D)
        )
        first = 1 if g == 0 else 0

        def dispatch(j, carry, g=g):
            remote(obuf.at[g, j], xbuf.at[g, tp, j], dsend.at[g], drecv.at[g], there(g, j, 1), tp).start()
            return carry

        lax.fori_loop(first, PEERS, dispatch, 0)
        if g == 0:
            xbuf[0, tp, 0] = obuf[0, 0]

    def arrived(g):
        first = 1 if isinstance(g, int) and g == 0 else 0
        part = xbuf.at[g, tp, pl.ds(first, PEERS - first)]
        remote(part, part, dsend.at[g], drecv.at[g], sp, other).wait_recv()
        remote(xbuf.at[g, tp], xbuf.at[g, tp], fsend.at[g], frecv.at[g], sp, other).start()

    def swap_of(g):
        return remote(ybuf.at[g, other], yrecv.at[g], ysendsem.at[g], yrecvsem.at[g], sp, other)

    def finish(g):
        swap_of(g).wait_recv()
        ybuf[g, tp] = (ybuf[g, tp].astype(F32) + yrecv[g].astype(F32)).astype(BF16)

        def send_back(j, carry):
            remote(ybuf.at[g, tp, j], back.at[g, j], bsend.at[g], brecv.at[g], there(g, j, -1), tp).start()
            return carry

        lax.fori_loop(jnp.where(g == 0, 1, 0), PEERS, send_back, 0)

    arrived(0)
    for load in loads[3:6]:
        load.wait()

    def group(g, carry):
        part = xbuf.at[g, other]
        remote(part, part, fsend.at[g], frecv.at[g], sp, other).wait_recv()
        lhs[...] = xbuf[g].reshape(TOK, D)
        gate = jnp.dot(lhs[...], wg[...], preferred_element_type=F32)
        up = jnp.dot(lhs[...], wu[...], preferred_element_type=F32)
        hid[...] = (gate / (1.0 + jnp.exp(-gate)) * up).astype(BF16)

        @pl.when(g > 0)
        def _():
            finish(g - 1)

        @pl.when(g + 1 < GROUPS)
        def _():
            arrived(g + 1)

        made = jnp.dot(hid[...], wd[...], preferred_element_type=F32).astype(BF16)
        ybuf[g] = made.reshape(2, PEERS, CAP, D)
        swap_of(g).start()
        return carry

    lax.fori_loop(0, GROUPS, group, 0)
    finish(GROUPS - 1)
    back[0, 0] = ybuf[0, tp, 0]

    combined = RESIDUAL_SCALE * nrm[...].astype(F32)
    picked = [jnp.zeros((ROWS, D), F32) for _ in range(TOPK)]
    for g in range(GROUPS):
        first = 1 if g == 0 else 0
        part = back.at[g, pl.ds(first, PEERS - first)]
        remote(part, part, bsend.at[g], brecv.at[g], sp, other).wait_recv()
        landed = back[g].reshape(ROWS, D)
        for k in range(TOPK):
            picked[k] = picked[k] + jnp.dot(
                gathers[k][:, g * ROWS : (g + 1) * ROWS], landed, preferred_element_type=F32
            )
    for k in range(TOPK):
        combined = combined + picked[k] * shares[k]
    out[...] = layer_norm(combined, last_gain[...]).astype(BF16)

    swap.wait_send()
    for d in range(REACH):
        for copy in (latent_sends[d], aux_sends[d], *relays(d, tp)):
            copy.wait_send()
    for g in range(GROUPS):
        first = 1 if g == 0 else 0
        part = obuf.at[g, pl.ds(first, PEERS - first)]
        remote(part, part, dsend.at[g], drecv.at[g], sp, other).wait_send()
        part = ybuf.at[g, tp, pl.ds(first, PEERS - first)]
        remote(part, part, bsend.at[g], brecv.at[g], sp, other).wait_send()
        remote(xbuf.at[g, tp], xbuf.at[g, tp], fsend.at[g], frecv.at[g], sp, other).wait_send()
        swap_of(g).wait_send()


def in_vmem():
    return pl.BlockSpec(memory_space=pltpu.VMEM)


def in_hbm():
    return pl.BlockSpec(memory_space=pltpu.HBM)


DMA = pltpu.SemaphoreType.DMA


def layer(*operands):
    return pl.pallas_call(
        layer_kernel,
        out_shape=jax.ShapeDtypeStruct((ROWS, D), BF16),
        in_specs=[in_vmem()] * 8 + [in_hbm()] * 9,
        out_specs=in_vmem(),
        scratch_shapes=[
            pltpu.VMEM((TOK, LOCAL_HEADS * DK), BF16),
            pltpu.VMEM((TOK, LOCAL_HEADS * DR), BF16),
            pltpu.VMEM((ROWS, D), BF16),
            pltpu.VMEM((TOK, 128), BF16),
            pltpu.VMEM((TOK, LOCAL_HEADS * 128), BF16),
            pltpu.VMEM((REACH, 2, ROWS, RANK), BF16),
            pltpu.VMEM((REACH, 2, ROWS, 128), BF16),
            pltpu.VMEM((RANK, LOCAL_HEADS * DK), BF16),
            pltpu.VMEM((RANK, LOCAL_HEADS * DV), BF16),
            pltpu.VMEM((LOCAL_HEADS * DV, D), BF16),
            pltpu.VMEM((LOCAL_HEADS, TOK, 128), F32),
            pltpu.VMEM((LOCAL_HEADS, TOK, 2 * DV), F32),
            pltpu.VMEM((TOK, LOCAL_HEADS * DV), BF16),
            pltpu.VMEM((ROWS, D), BF16),
            pltpu.VMEM((ROWS, D), BF16),
            pltpu.VMEM((ROWS, D), BF16),
            pltpu.VMEM((D, FFH), BF16),
            pltpu.VMEM((D, FFH), BF16),
            pltpu.VMEM((FFH, D), BF16),
            pltpu.VMEM((GROUPS, PEERS, CAP, D), BF16),
            pltpu.VMEM((GROUPS, 2, PEERS, CAP, D), BF16),
            pltpu.VMEM((TOK, D), BF16),
            pltpu.VMEM((TOK, FFH), BF16),
            pltpu.VMEM((GROUPS, 2, PEERS, CAP, D), BF16),
            pltpu.VMEM((GROUPS, PEERS, CAP, D), BF16),
            pltpu.VMEM((GROUPS, PEERS, CAP, D), BF16),
            DMA((9,)),
        ]
        + [DMA((2, REACH))] * 4
        + [DMA((2,)), pltpu.SemaphoreType.REGULAR((2,))]
        + [DMA((GROUPS,))] * 8,
        compiler_params=pltpu.CompilerParams(
            collective_id=0, has_side_effects=True, vmem_limit_bytes=VMEM_LIMIT
        ),
    )(*operands)


def per_device(
    latent,
    rotary_key,
    doc_ids,
    queries_content,
    queries_rotary,
    w_key_up,
    w_value_up,
    w_out,
    residual,
    norm_gain,
    routes,
    route_weights,
    w_gate,
    w_up,
    w_down,
    out_gain,
):
    frequency = jnp.asarray(np.tile(ROPE_THETA ** (-2.0 * np.arange(DR // 2) / DR), 4), F32)
    mixed = layer(
        latent,
        rotary_key.T,
        doc_ids.reshape(1, TOK),
        frequency.reshape(1, 128),
        norm_gain.reshape(1, D),
        routes.T,
        route_weights.T,
        out_gain.reshape(1, D),
        queries_content,
        queries_rotary,
        residual,
        w_key_up,
        w_value_up,
        w_out,
        w_gate,
        w_up,
        w_down,
    )
    return mixed


def solution(mesh):
    return jax.shard_map(
        per_device,
        mesh=mesh,
        in_specs=(
            P("sp", None),
            P("sp", None),
            P("sp"),
            P("sp", "tp"),
            P("sp", "tp"),
            P(),
            P(),
            P("tp", None),
            P(("sp", "tp"), None),
            P(),
            P(("sp", "tp"), None),
            P(("sp", "tp"), None),
            P("sp", None, "tp"),
            P("sp", None, "tp"),
            P("sp", "tp", None),
            P(),
        ),
        out_specs=P(("sp", "tp"), None),
        check_vma=False,
    )
```

time: 113 us -> 87.2 us (0.77)
  the two profiles are of different devices: /device:TPU:1 before, /device:TPU:3 now
where the time goes in v2:
time: 87.2 us; the launch traced here: 87.1 us
  Pallas kernels  85.2 us (98%)
  local copies, waits for them, and re-layouts  1.88 us (2%)
    pallas_call x1, Pallas kernels, layer(): pl.pallas_call(layer_kernel, out_shape=jax.ShapeDtypeStruct((ROWS, D), BF...  85.2 us
    unnamed x1, local copies, waits for them, and re-layouts  1.88 us

profile of v2, /device:TPU:3, one launch (start us, length us, event | category | flops | bytes accessed | tf_op | source)
XLA Modules:
  0.0 87.1 jit_solution(11670400295487862868)
XLA Ops:
  0.0 85.2 %shard_map.163 = bf16[128,2048]{1,0:T(8,128)(2,1)} custom-call(bf16[256,256]{1,0:T(8,128)(2,1)} %latent.1, bf16[64,256]{1,0:T(8,128)(2,1)} %bitcast.6, s32[1,256]{1,0:T(1,128)} %bitcast.9, f32[1,128]{1,0:T(1,128)} %constant.6.frequency, f32[1,2048]{1,0:T(1,128)} %bitcast.7, s32[2,128]{1,0:T(2,128)} %bitcast.10, f32[2,128]{1,0:T(2,128)} %bitcast.11, ...), custom_call_target="tpu_custom_call" | custom-call | tf_op jit(solution)/shard_map/pallas_call | solution.py:396
  85.2 1.9 %copy.19 = bf16[128,2048]{1,0:T(8,128)(2,1)} copy(bf16[128,2048]{1,0:T(8,128)(2,1)} %shard_map.163) | data formatting | bytes 1048576

commit v3 on v2

--- a/solution.py
+++ b/solution.py
@@ -76,7 +76,8 @@
     wv,
     wo,
     peaks,
-    sums,
+    scores,
+    vals,
     att,
     psend,
     precv,
@@ -142,11 +143,30 @@
     mine = pl.ds(pl.multiple_of(tp * ROWS, ROWS), ROWS)
     theirs = pl.ds(pl.multiple_of(other * ROWS, ROWS), ROWS)
     pl.semaphore_wait(barrier, 18)
-    latent_sends = []
-    for d in range(REACH):
-        chip = lax.rem(sp + d + 1, CHIPS)
-        latent_sends.append(remote(latent.at[mine], kvl.at[d, tp], ssem.at[0, d], rsem.at[0, d], chip, tp))
-        latent_sends[-1].start()
+
+    def passed_on(d):
+        return (tp == 1) & (x + d + 1 >= 4)
+
+    def block_send(i, src, d, chip):
+        part = (kvl, kva)[i]
+        return remote(src, part.at[d, tp], ssem.at[i, d], rsem.at[i, d], chip, tp)
+
+    def send_own(i, src):
+        block_send(i, src.at[mine], REACH - 1, lax.rem(sp + REACH, CHIPS)).start()
+        for d in range(REACH - 1):
+
+            @pl.when(jnp.logical_not(passed_on(d)))
+            def _(d=d):
+                block_send(i, src.at[mine], d, lax.rem(sp + d + 1, CHIPS)).start()
+
+    def pass_on(i):
+        for d in range(REACH - 1):
+
+            @pl.when(passed_on(d))
+            def _(d=d):
+                block_send(i, (kvl, kva)[i].at[REACH - 1, tp], d, x_ring[d]).start()
+
+    send_own(0, latent)
 
     doc_lane = lax.broadcasted_iota(jnp.int32, (64, TOK), 0)
     marks = (doc_lane == doc_row[...]).astype(F32)
@@ -164,11 +184,7 @@
         return v * cos_table + swapped * sin_table
 
     aux_out[...] = jnp.where(content, turned(natural), natural).astype(BF16)
-    aux_sends = []
-    for d in range(REACH):
-        chip = lax.rem(sp + d + 1, CHIPS)
-        aux_sends.append(remote(aux_out.at[mine], kva.at[d, tp], ssem.at[1, d], rsem.at[1, d], chip, tp))
-        aux_sends[-1].start()
+    send_own(1, aux_out)
     loads[7].wait()
     fence = jnp.where(wide < DR + 32, (natural - 1.0) * -EXCLUDED, 0.0)
     for pair in range(LOCAL_HEADS // 2):
@@ -216,32 +232,26 @@
         load.start()
 
     rate = (DK + DR) ** (-0.5) * LOG2E
-    ones = jnp.ones((TOK, DV), BF16)
-
-    def block(lat, aux, first):
+    ones = jnp.ones(((REACH + 1) * TOK, DV), BF16)
+
+    def block(lat, aux, slot):
+        span = slice(slot * TOK, (slot + 1) * TOK)
         keys = jnp.dot(lat, wk[...], preferred_element_type=F32).astype(BF16)
-        values = jnp.dot(lat, wv[...], preferred_element_type=F32).astype(BF16)
+        vals[span, :] = jnp.dot(lat, wv[...], preferred_element_type=F32).astype(BF16)
         for h in range(LOCAL_HEADS):
             hs = slice(h * DK, (h + 1) * DK)
             query = jnp.concatenate([qc[:, hs], qaux[:, hs]], 1)
             key = jnp.concatenate([keys[:, hs], aux], 1)
             s = lax.dot_general(query, key, (((1,), (1,)), ((), ())), preferred_element_type=F32)
-            if first:
+            if slot == 0:
                 r = lax.broadcasted_iota(jnp.int32, (TOK, TOK), 0)
                 c = lax.broadcasted_iota(jnp.int32, (TOK, TOK), 1)
                 s = jnp.where(c <= r, s, EXCLUDED)
-            peak = jnp.max(s, -1, keepdims=True)
-            if not first:
-                was = peaks[h][:, :1]
-                peak = jnp.maximum(peak, was)
-            lifted = jnp.exp2((s - peak) * rate).astype(BF16)
-            made = jnp.dot(lifted, jnp.concatenate([values[:, hs], ones], 1), preferred_element_type=F32)
-            if not first:
-                made = made + sums[h] * jnp.exp2((was - peak) * rate)
-            peaks[h] = jnp.broadcast_to(peak, (TOK, 128))
-            sums[h] = made
-
-    block(latent[...], aux_out[...], True)
+            scores[h, :, span] = s
+            peak = jnp.maximum(s[:, :128], s[:, 128:])
+            peaks[h] = peak if slot == 0 else jnp.maximum(peaks[h], peak)
+
+    block(latent[...], aux_out[...], 0)
     pl.semaphore_wait(met.at[0], 3)
     for chip in z_ring:
         signal(met.at[1], chip, tp)
@@ -255,20 +265,27 @@
     def process(d):
         for relay in relays(d, other):
             relay.wait_recv()
-        block(kvl[d].reshape(TOK, RANK), kva[d].reshape(TOK, 128), False)
-
-    for d in range(REACH):
-        for send, relay in zip((latent_sends[d], aux_sends[d]), relays(d, tp)):
-            send.wait_recv()
+        block(kvl[d].reshape(TOK, RANK), kva[d].reshape(TOK, 128), d + 1)
+
+    order = (REACH - 1, 0, 1, 2)
+    for n, d in enumerate(order):
+        for i, relay in enumerate(relays(d, tp)):
+            block_send(i, (kvl, kva)[i].at[d, tp], d, near[3]).wait_recv()
+            if n == 0:
+                pass_on(i)
             relay.start()
-        if d >= 1:
-            process(d - 1)
+        if n >= 1:
+            process(order[n - 1])
     loads[2].wait()
     loads[8].wait()
-    process(REACH - 1)
+    process(order[-1])
 
     for h in range(LOCAL_HEADS):
-        att[:, h * DV : (h + 1) * DV] = (sums[h, :, :DV] / sums[h, :, DV:]).astype(BF16)
+        hs = slice(h * DV, (h + 1) * DV)
+        peak = jnp.max(peaks[h], -1, keepdims=True)
+        lifted = jnp.exp2((scores[h] - peak) * rate).astype(BF16)
+        made = jnp.dot(lifted, jnp.concatenate([vals[:, hs], ones], 1), preferred_element_type=F32)
+        att[:, hs] = (made[:, :DV] / made[:, DV:]).astype(BF16)
     psend[...] = jnp.dot(att[theirs, :], wo[...], preferred_element_type=F32).astype(BF16)
     swap = remote(psend, precv, psem.at[0], psem.at[1], sp, other)
     swap.start()
@@ -369,8 +386,9 @@
 
     swap.wait_send()
     for d in range(REACH):
-        for copy in (latent_sends[d], aux_sends[d], *relays(d, tp)):
-            copy.wait_send()
+        for i, relay in enumerate(relays(d, tp)):
+            block_send(i, (kvl, kva)[i].at[d, tp], d, near[3]).wait_send()
+            relay.wait_send()
     for g in range(GROUPS):
         first = 1 if g == 0 else 0
         part = obuf.at[g, pl.ds(first, PEERS - first)]
@@ -410,7 +428,8 @@
             pltpu.VMEM((RANK, LOCAL_HEADS * DV), BF16),
             pltpu.VMEM((LOCAL_HEADS * DV, D), BF16),
             pltpu.VMEM((LOCAL_HEADS, TOK, 128), F32),
-            pltpu.VMEM((LOCAL_HEADS, TOK, 2 * DV), F32),
+            pltpu.VMEM((LOCAL_HEADS, TOK, (REACH + 1) * TOK), F32),
+            pltpu.VMEM(((REACH + 1) * TOK, LOCAL_HEADS * DV), BF16),
             pltpu.VMEM((TOK, LOCAL_HEADS * DV), BF16),
             pltpu.VMEM((ROWS, D), BF16),
             pltpu.VMEM((ROWS, D), BF16),

time: 87.2 us -> 82.7 us (0.948)
  the two profiles are of different devices: /device:TPU:3 before, /device:TPU:12 now
where the time goes in v3:
time: 82.7 us; the launch traced here: 82.3 us
  Pallas kernels  80.4 us (97%)
  local copies, waits for them, and re-layouts  1.88 us (2%)
    pallas_call x1, Pallas kernels, layer(): pl.pallas_call(layer_kernel, out_shape=jax.ShapeDtypeStruct((ROWS, D), BF...  80.4 us
    unnamed x1, local copies, waits for them, and re-layouts  1.88 us

profile of v3, /device:TPU:12, one launch (start us, length us, event | category | flops | bytes accessed | tf_op | source)
XLA Modules:
  0.0 82.3 jit_solution(6584180403269451702)
XLA Ops:
  0.0 80.4 %shard_map.163 = bf16[128,2048]{1,0:T(8,128)(2,1)} custom-call(bf16[256,256]{1,0:T(8,128)(2,1)} %latent.1, bf16[64,256]{1,0:T(8,128)(2,1)} %bitcast.6, s32[1,256]{1,0:T(1,128)} %bitcast.9, f32[1,128]{1,0:T(1,128)} %constant.6.frequency, f32[1,2048]{1,0:T(1,128)} %bitcast.7, s32[2,128]{1,0:T(2,128)} %bitcast.10, f32[2,128]{1,0:T(2,128)} %bitcast.11, ...), custom_call_target="tpu_custom_call" | custom-call | tf_op jit(solution)/shard_map/pallas_call | solution.py:414
  80.4 1.9 %copy.19 = bf16[128,2048]{1,0:T(8,128)(2,1)} copy(bf16[128,2048]{1,0:T(8,128)(2,1)} %shard_map.163) | data formatting | bytes 1048576

commit v4 on v3

--- a/solution.py
+++ b/solution.py
@@ -47,14 +47,14 @@
 
 
 def layer_kernel(
-    latent,
-    key_rot,
-    doc_row,
-    frequency,
-    gain,
-    routes,
-    weights,
-    last_gain,
+    latent_hbm,
+    key_rot_hbm,
+    doc_row_hbm,
+    frequency_hbm,
+    gain_hbm,
+    routes_hbm,
+    weights_hbm,
+    last_gain_hbm,
     qc_hbm,
     qr_hbm,
     residual_hbm,
@@ -65,6 +65,14 @@
     wu_hbm,
     wd_hbm,
     out,
+    latent,
+    key_rot,
+    doc_row,
+    frequency,
+    gain,
+    routes,
+    weights,
+    last_gain,
     qc,
     qr,
     residual,
@@ -79,8 +87,7 @@
     scores,
     vals,
     att,
-    psend,
-    precv,
+    att_in,
     nrm,
     wg,
     wu,
@@ -92,6 +99,7 @@
     ybuf,
     yrecv,
     back,
+    small_sem,
     wsem,
     ssem,
     rsem,
@@ -125,12 +133,29 @@
         signal(barrier, chip, tp)
     signal(barrier, sp, other)
 
+    small = [
+        pltpu.make_async_copy(src, dst, small_sem.at[k])
+        for k, (src, dst) in enumerate(
+            (
+                (latent_hbm, latent),
+                (key_rot_hbm, key_rot),
+                (doc_row_hbm, doc_row),
+                (frequency_hbm, frequency),
+                (gain_hbm, gain),
+                (routes_hbm, routes),
+                (weights_hbm, weights),
+                (last_gain_hbm, last_gain),
+            )
+        )
+    ]
+    for load in small:
+        load.start()
     half = LOCAL_HEADS * DK
     cols = pl.ds(pl.multiple_of(tp * half, half), half)
     loads = [
         pltpu.make_async_copy(wk_hbm.at[:, cols], wk, wsem.at[0]),
         pltpu.make_async_copy(wv_hbm.at[:, cols], wv, wsem.at[1]),
-        pltpu.make_async_copy(wo_hbm, wo, wsem.at[2]),
+        pltpu.make_async_copy(wo_hbm, wo.at[tp], wsem.at[2]),
         pltpu.make_async_copy(wg_hbm.at[0], wg, wsem.at[3]),
         pltpu.make_async_copy(wu_hbm.at[0], wu, wsem.at[4]),
         pltpu.make_async_copy(wd_hbm.at[0], wd, wsem.at[5]),
@@ -142,6 +167,8 @@
         loads[k].start()
     mine = pl.ds(pl.multiple_of(tp * ROWS, ROWS), ROWS)
     theirs = pl.ds(pl.multiple_of(other * ROWS, ROWS), ROWS)
+    for load in small:
+        load.wait()
     pl.semaphore_wait(barrier, 18)
 
     def passed_on(d):
@@ -153,20 +180,23 @@
 
     def send_own(i, src):
         block_send(i, src.at[mine], REACH - 1, lax.rem(sp + REACH, CHIPS)).start()
-        for d in range(REACH - 1):
+        for d in (2, 1, 0):
 
             @pl.when(jnp.logical_not(passed_on(d)))
             def _(d=d):
                 block_send(i, src.at[mine], d, lax.rem(sp + d + 1, CHIPS)).start()
 
     def pass_on(i):
-        for d in range(REACH - 1):
+        for d in (2, 1, 0):
 
             @pl.when(passed_on(d))
             def _(d=d):
                 block_send(i, (kvl, kva)[i].at[REACH - 1, tp], d, x_ring[d]).start()
 
     send_own(0, latent)
+    loads[2].wait()
+    share = remote(wo.at[tp], wo.at[tp], psem.at[2], psem.at[3], sp, other)
+    share.start()
 
     doc_lane = lax.broadcasted_iota(jnp.int32, (64, TOK), 0)
     marks = (doc_lane == doc_row[...]).astype(F32)
@@ -267,7 +297,7 @@
             relay.wait_recv()
         block(kvl[d].reshape(TOK, RANK), kva[d].reshape(TOK, 128), d + 1)
 
-    order = (REACH - 1, 0, 1, 2)
+    order = (REACH - 1, 2, 1, 0)
     for n, d in enumerate(order):
         for i, relay in enumerate(relays(d, tp)):
             block_send(i, (kvl, kva)[i].at[d, tp], d, near[3]).wait_recv()
@@ -276,7 +306,6 @@
             relay.start()
         if n >= 1:
             process(order[n - 1])
-    loads[2].wait()
     loads[8].wait()
     process(order[-1])
 
@@ -286,13 +315,14 @@
         lifted = jnp.exp2((scores[h] - peak) * rate).astype(BF16)
         made = jnp.dot(lifted, jnp.concatenate([vals[:, hs], ones], 1), preferred_element_type=F32)
         att[:, hs] = (made[:, :DV] / made[:, DV:]).astype(BF16)
-    psend[...] = jnp.dot(att[theirs, :], wo[...], preferred_element_type=F32).astype(BF16)
-    swap = remote(psend, precv, psem.at[0], psem.at[1], sp, other)
+    swap = remote(att.at[theirs], att_in, psem.at[0], psem.at[1], sp, other)
     swap.start()
-    own = jnp.dot(att[mine, :], wo[...], preferred_element_type=F32).astype(BF16).astype(F32)
+    own = jnp.dot(att[mine, :], wo[tp], preferred_element_type=F32).astype(BF16).astype(F32)
     own = own + RESIDUAL_SCALE * residual[...].astype(F32)
+    remote(wo.at[other], wo.at[other], psem.at[2], psem.at[3], sp, other).wait_recv()
     swap.wait_recv()
-    rows_in = layer_norm(own + precv[...].astype(F32), gain[...]).astype(BF16)
+    rest = jnp.dot(att_in[...], wo[other], preferred_element_type=F32).astype(BF16).astype(F32)
+    rows_in = layer_norm(own + rest, gain[...]).astype(BF16)
     nrm[...] = rows_in
 
     def there(g, j, sign):
@@ -314,6 +344,7 @@
         first = 1 if g == 0 else 0
 
         def dispatch(j, carry, g=g):
+            j = jnp.where(tp == 1, PEERS - 1 + (1 if g == 0 else 0) - j, j)
             remote(obuf.at[g, j], xbuf.at[g, tp, j], dsend.at[g], drecv.at[g], there(g, j, 1), tp).start()
             return carry
 
@@ -335,6 +366,7 @@
         ybuf[g, tp] = (ybuf[g, tp].astype(F32) + yrecv[g].astype(F32)).astype(BF16)
 
         def send_back(j, carry):
+            j = jnp.where(tp == 1, PEERS - 1 + jnp.where(g == 0, 1, 0) - j, j)
             remote(ybuf.at[g, tp, j], back.at[g, j], bsend.at[g], brecv.at[g], there(g, j, -1), tp).start()
             return carry
 
@@ -385,6 +417,7 @@
     out[...] = layer_norm(combined, last_gain[...]).astype(BF16)
 
     swap.wait_send()
+    share.wait_send()
     for d in range(REACH):
         for i, relay in enumerate(relays(d, tp)):
             block_send(i, (kvl, kva)[i].at[d, tp], d, near[3]).wait_send()
@@ -414,9 +447,17 @@
     return pl.pallas_call(
         layer_kernel,
         out_shape=jax.ShapeDtypeStruct((ROWS, D), BF16),
-        in_specs=[in_vmem()] * 8 + [in_hbm()] * 9,
+        in_specs=[in_hbm()] * 17,
         out_specs=in_vmem(),
         scratch_shapes=[
+            pltpu.VMEM((TOK, RANK), BF16),
+            pltpu.VMEM((DR, TOK), BF16),
+            pltpu.VMEM((1, TOK), jnp.int32),
+            pltpu.VMEM((1, 128), F32),
+            pltpu.VMEM((1, D), F32),
+            pltpu.VMEM((TOPK, ROWS), jnp.int32),
+            pltpu.VMEM((TOPK, ROWS), F32),
+            pltpu.VMEM((1, D), F32),
             pltpu.VMEM((TOK, LOCAL_HEADS * DK), BF16),
             pltpu.VMEM((TOK, LOCAL_HEADS * DR), BF16),
             pltpu.VMEM((ROWS, D), BF16),
@@ -426,13 +467,12 @@
             pltpu.VMEM((REACH, 2, ROWS, 128), BF16),
             pltpu.VMEM((RANK, LOCAL_HEADS * DK), BF16),
             pltpu.VMEM((RANK, LOCAL_HEADS * DV), BF16),
-            pltpu.VMEM((LOCAL_HEADS * DV, D), BF16),
+            pltpu.VMEM((2, LOCAL_HEADS * DV, D), BF16),
             pltpu.VMEM((LOCAL_HEADS, TOK, 128), F32),
             pltpu.VMEM((LOCAL_HEADS, TOK, (REACH + 1) * TOK), F32),
             pltpu.VMEM(((REACH + 1) * TOK, LOCAL_HEADS * DV), BF16),
             pltpu.VMEM((TOK, LOCAL_HEADS * DV), BF16),
-            pltpu.VMEM((ROWS, D), BF16),
-            pltpu.VMEM((ROWS, D), BF16),
+            pltpu.VMEM((ROWS, LOCAL_HEADS * DV), BF16),
             pltpu.VMEM((ROWS, D), BF16),
             pltpu.VMEM((D, FFH), BF16),
             pltpu.VMEM((D, FFH), BF16),
@@ -444,10 +484,11 @@
             pltpu.VMEM((GROUPS, 2, PEERS, CAP, D), BF16),
             pltpu.VMEM((GROUPS, PEERS, CAP, D), BF16),
             pltpu.VMEM((GROUPS, PEERS, CAP, D), BF16),
+            DMA((8,)),
             DMA((9,)),
         ]
         + [DMA((2, REACH))] * 4
-        + [DMA((2,)), pltpu.SemaphoreType.REGULAR((2,))]
+        + [DMA((4,)), pltpu.SemaphoreType.REGULAR((2,))]
         + [DMA((GROUPS,))] * 8,
         compiler_params=pltpu.CompilerParams(
             collective_id=0, has_side_effects=True, vmem_limit_bytes=VMEM_LIMIT

time: 82.7 us -> 80.9 us (0.978)
  Pallas kernels: 80.4 us -> 78.9 us
    pallas_call x1, Pallas kernels: 80.4 us -> 78.9 us  [layer(): pl.pallas_call(layer_kernel, out_shape=jax.ShapeDtypeStruct((ROWS, D), BF...]
where the time goes in v4:
time: 80.9 us; the launch traced here: 80.8 us
  Pallas kernels  78.9 us (98%)
  local copies, waits for them, and re-layouts  1.88 us (2%)
    pallas_call x1, Pallas kernels, layer(): pl.pallas_call(layer_kernel, out_shape=jax.ShapeDtypeStruct((ROWS, D), BF...  78.9 us
    unnamed x1, local copies, waits for them, and re-layouts  1.88 us

profile of v4, /device:TPU:12, one launch (start us, length us, event | category | flops | bytes accessed | tf_op | source)
XLA Modules:
  0.0 80.8 jit_solution(10202740349091679240)
XLA Ops:
  0.0 78.9 %shard_map.163 = bf16[128,2048]{1,0:T(8,128)(2,1)} custom-call(bf16[256,256]{1,0:T(8,128)(2,1)} %latent_hbm.1, bf16[64,256]{1,0:T(8,128)(2,1)} %bitcast.6, s32[1,256]{1,0:T(1,128)} %bitcast.9, f32[1,128]{1,0:T(1,128)} %constant.6.frequency_hbm, f32[1,2048]{1,0:T(1,128)} %bitcast.7, s32[2,128]{1,0:T(2,128)} %bitcast.10, f32[2,128]{1,0:T(2,128)} %bitcast.11, ...), custom_call_target="tpu_custom_call" | custom-call | tf_op jit(solution)/shard_map/pallas_call | solution.py:447
  78.9 1.9 %copy.19 = bf16[128,2048]{1,0:T(8,128)(2,1)} copy(bf16[128,2048]{1,0:T(8,128)(2,1)} %shard_map.163) | data formatting | bytes 1048576

commit v5 on v4

--- a/solution.py
+++ b/solution.py
@@ -384,13 +384,13 @@
         up = jnp.dot(lhs[...], wu[...], preferred_element_type=F32)
         hid[...] = (gate / (1.0 + jnp.exp(-gate)) * up).astype(BF16)
 
+        @pl.when(g + 1 < GROUPS)
+        def _():
+            arrived(g + 1)
+
         @pl.when(g > 0)
         def _():
             finish(g - 1)
-
-        @pl.when(g + 1 < GROUPS)
-        def _():
-            arrived(g + 1)
 
         made = jnp.dot(hid[...], wd[...], preferred_element_type=F32).astype(BF16)
         ybuf[g] = made.reshape(2, PEERS, CAP, D)

time: 80.9 us -> 81.2 us (level)
  no operation moved by 1% of the time
where the time goes in v5:
time: 81.2 us; the launch traced here: 81.1 us
  Pallas kernels  79.2 us (98%)
  local copies, waits for them, and re-layouts  1.88 us (2%)
    pallas_call x1, Pallas kernels, layer(): pl.pallas_call(layer_kernel, out_shape=jax.ShapeDtypeStruct((ROWS, D), BF...  79.2 us
    unnamed x1, local copies, waits for them, and re-layouts  1.88 us

profile of v5, /device:TPU:12, one launch (start us, length us, event | category | flops | bytes accessed | tf_op | source)
XLA Modules:
  0.0 81.1 jit_solution(1229941708709656594)
XLA Ops:
  0.0 79.2 %shard_map.163 = bf16[128,2048]{1,0:T(8,128)(2,1)} custom-call(bf16[256,256]{1,0:T(8,128)(2,1)} %latent_hbm.1, bf16[64,256]{1,0:T(8,128)(2,1)} %bitcast.6, s32[1,256]{1,0:T(1,128)} %bitcast.9, f32[1,128]{1,0:T(1,128)} %constant.6.frequency_hbm, f32[1,2048]{1,0:T(1,128)} %bitcast.7, s32[2,128]{1,0:T(2,128)} %bitcast.10, f32[2,128]{1,0:T(2,128)} %bitcast.11, ...), custom_call_target="tpu_custom_call" | custom-call | tf_op jit(solution)/shard_map/pallas_call | solution.py:447
  79.2 1.9 %copy.19 = bf16[128,2048]{1,0:T(8,128)(2,1)} copy(bf16[128,2048]{1,0:T(8,128)(2,1)} %shard_map.163) | data formatting | bytes 1048576
